TPU v7x, 512 devices: a whole 4x8x8 slice. The times are simulated.
512 devices in a mesh: dp: 4 (over x), kv: 64 (over z, y), tp: 2 (over core).
Axes of the slice: x: 4, y: 8, z: 8, core: 2. Of those that a mesh axis runs over, the one named last changes fastest.
Arguments:
- tokens: bfloat16 [24, 4096], P('dp', 'kv'), may hold values from -64 to 64
- lengths: int32 [24], P('dp'), may hold values from 2048 to 16384, as said below
- attn_gain: float32 [4096], P('kv'), may hold values from 0.1 to 1.9
- query_weight: bfloat16 [4096, 4096], P('kv', 'tp'), may hold values from -0.09375 to 0.09375
- key_weight: bfloat16 [4096, 256], P('kv', 'tp'), may hold values from -0.1875 to 0.1875
- value_weight: bfloat16 [4096, 256], P('kv', 'tp'), may hold values from -0.09375 to 0.09375
- forget_weight: bfloat16 [4096, 4], replicated, may hold values from -0.25 to 0.25
- forget_offset: float32 [4], P('tp'), may hold values from -6 to 0
- cache_keys: bfloat16 [24, 16384, 256], P('dp', 'kv', 'tp'), may hold values from -1600 to 1600
- cache_values: bfloat16 [24, 16384, 256], P('dp', 'kv', 'tp'), may hold values from -6 to 6
- gate_sum: float32 [24, 4, 16384], P('dp', 'tp', 'kv'), may hold values from -1264 to 0
- out_weight: bfloat16 [4096, 4096], P('tp', 'kv'), may hold values from -0.1875 to 0.1875
- mlp_gain: float32 [4096], replicated, may hold values from 0.1 to 1.9
- up_weight: bfloat16 [4096, 16384], P(None, ('kv', 'tp')), may hold values from -0.09375 to 0.09375
- down_weight: bfloat16 [16384, 4096], P(('kv', 'tp')), may hold values from -0.1875 to 0.1875
Outputs:
- mixed: bfloat16 [24, 4096], P('dp', ('kv', 'tp'))
Inputs may be any that keep to these rules, and one draw needn't show every extreme that they name: `lengths`: in every draw some sequence has all 16384 positions cached.
All inputs are finite; a program needn't handle non-finite values.
Results may differ from a plain program's by a relative error of at most 0.023.
Values may be sent and summed in bfloat16 or wider, within the bound.
No kernel may reach another device: no remote copies, remote signals or barrier semaphores. Data moves between devices by JAX's collectives and lax.ppermute only.
A program may use at most 64 MiB of HBM per device.

v0:
```python
import functools

import jax
import jax.numpy as jnp
from jax import lax
from jax.sharding import Mesh
from jax.sharding import PartitionSpec as P

D = 4096
HEADS = 64
HD = 64
KEY_VALUE_HEADS = 4
KV = ("kv_0", "kv_1")
KV_TP = ("kv_0", "kv_1", "tp")


epsilon = 1e-06
floor_score = -1e30


def over_axes(x, axes):
    return functools.reduce(lax.psum, axes, x)


def gathered_once(x, axis):
    leaves = jax.tree.leaves(x)
    order = sorted(range(len(leaves)), key=lambda k: -leaves[k].size)
    width = (1, *leaves[order[0]].shape)[-1]
    lines = [
        jnp.pad(leaves[k].reshape(-1), (0, -leaves[k].size % width)).reshape(-1, width)
        for k in order
    ]
    both, at, found = (lax.all_gather(jnp.concatenate(lines), axis), 0, {})
    for k, line in zip(order, lines):
        section = both[:, at : at + len(line)].reshape(len(both), -1)
        found[k] = section[:, : leaves[k].size].reshape(-1, *leaves[k].shape)
        at += len(line)
    numbers = iter(range(len(leaves)))
    return jax.tree.map(lambda _: found[next(numbers)], x)


def combined_by_axis(x, axes, combine):
    for axis in axes:
        pieces = gathered_once(
            jax.tree.map(
                lambda part, kind: part.astype(kind), x, (jnp.bfloat16, jnp.bfloat16, jnp.bfloat16)
            ),
            axis,
        )
        widened = [
            jax.tree.map(lambda part, own: part[k].astype(own.dtype), pieces, x)
            for k in range(lax.axis_size(axis))
        ]
        x = widened[0]
        for theirs in widened[1:]:
            x = combine(x, theirs)
    return x


def over_pieces(x, axis):
    pieces = lax.all_gather(x, axis).astype(jnp.float32)
    return pieces.sum(axis=0)


def from_everyone(x, axis):
    copies = jnp.broadcast_to(x, (lax.axis_size(axis), *x.shape))
    return lax.all_to_all(copies, axis, split_axis=0, concat_axis=0, tiled=True)


def in_order(pieces, dim):
    pieces = jnp.moveaxis(pieces, 0, dim)
    dims = pieces.shape
    return pieces.reshape(*dims[:dim], dims[dim] * dims[dim + 1], *dims[dim + 2 :])


def gathered_copies(x, axis, dim):
    pieces = from_everyone(x, axis)
    return in_order(pieces, dim)


def cut_along(x, dim, devices):
    dims = x.shape
    pieces = x.reshape(*dims[:dim], devices, dims[dim] // devices, *dims[dim + 1 :])
    return jnp.moveaxis(pieces, dim, 0)


def sent_and_summed(x, axis, dim):
    devices = lax.axis_size(axis)
    pieces = lax.all_to_all(cut_along(x, dim, devices), axis, 0, 0, tiled=True)
    return jnp.sum(pieces.astype(jnp.float32), axis=0)


def sum_at_owner(x, axis, dim):
    pieces = cut_along(x, dim, lax.axis_size(axis))
    arrived = lax.all_to_all(pieces, axis, split_axis=0, concat_axis=0, tiled=True)
    return arrived.sum(axis=0)


def combine_parts(earlier, later):
    first_top, first_total, first_values = earlier
    second_top, second_total, second_values = later
    merged_top = jnp.maximum(first_top, second_top)
    first_scale = jnp.exp(first_top - merged_top)
    second_scale = jnp.exp(second_top - merged_top)
    first_wide = jnp.repeat(first_scale, HD, axis=1)
    second_wide = jnp.repeat(second_scale, HD, axis=1)
    return (
        merged_top,
        first_total * first_scale + second_total * second_scale,
        first_values * first_wide + second_values * second_wide,
    )


def shards(
    tokens,
    lengths,
    attn_gain,
    query_weight,
    key_weight,
    value_weight,
    forget_weight,
    forget_offset,
    cache_keys,
    cache_values,
    gate_sum,
    out_weight,
    mlp_gain,
    up_weight,
    down_weight,
):
    row_count = tokens.shape[0]
    feature_cols = tokens.shape[1]
    kv_place = lax.axis_index(KV)
    tp_place = lax.axis_index("tp")
    local_heads = key_weight.shape[1] // HD
    group_size = HEADS // KEY_VALUE_HEADS
    token_rows = tokens.astype(jnp.float32)
    scaled_rows = (token_rows * attn_gain[None, :]).astype(jnp.bfloat16)
    square_part = jnp.sum(token_rows * token_rows, axis=1)
    query_part = jnp.dot(scaled_rows, query_weight, preferred_element_type=jnp.float32)
    key_part = jnp.dot(scaled_rows, key_weight, preferred_element_type=jnp.float32)
    value_part = jnp.dot(scaled_rows, value_weight, preferred_element_type=jnp.float32)
    gate_rows = lax.dynamic_slice(
        forget_weight,
        (kv_place * feature_cols, tp_place * local_heads),
        (feature_cols, local_heads),
    )
    forget_part = jnp.dot(scaled_rows, gate_rows, preferred_element_type=jnp.float32)
    query_sum, key_sum, value_sum, forget_sum, square_sum = (
        over_axes(query_part.astype(jnp.bfloat16), KV).astype(jnp.float32),
        over_axes(key_part.astype(jnp.bfloat16), KV).astype(jnp.float32),
        over_axes(value_part.astype(jnp.bfloat16), KV).astype(jnp.float32),
        over_axes(forget_part.astype(jnp.bfloat16), KV).astype(jnp.float32),
        over_axes(square_part.astype(jnp.bfloat16), KV).astype(jnp.float32),
    )
    row_scale = lax.rsqrt(square_sum / D + epsilon)[:, None]
    queries = (query_sum * row_scale).astype(jnp.bfloat16)
    new_key = (key_sum * row_scale).astype(jnp.bfloat16)
    new_value = (value_sum * row_scale).astype(jnp.bfloat16)
    log_forget = jax.nn.log_sigmoid(forget_sum * row_scale + forget_offset[None, :])
    positions_here = cache_keys.shape[1]
    key_heads = cache_keys.reshape(row_count, positions_here, local_heads, HD)
    value_heads = cache_values.reshape(row_count, positions_here, local_heads, HD)
    query_heads = queries.reshape(row_count, local_heads, group_size, HD)
    scores = jnp.einsum(
        "skgd,spkd->skgp", query_heads, key_heads, preferred_element_type=jnp.float32
    ) * HD ** (-0.5)
    scores = scores + gate_sum[:, :, None, :] + log_forget[:, :, None, None]
    cache_pos = kv_place * positions_here + jnp.arange(positions_here)
    active_mask = (cache_pos[None, :] < lengths[:, None])[:, None, None, :]
    local_top = jnp.max(jnp.where(active_mask, scores, floor_score), axis=3)
    weights = jnp.where(active_mask, jnp.exp(scores - local_top[..., None]), 0.0)
    local_total = jnp.sum(weights, axis=3)
    local_values = jnp.einsum(
        "skgp,spkd->skgd",
        weights.astype(jnp.bfloat16),
        value_heads,
        preferred_element_type=jnp.float32,
    )
    head_cols = local_heads * group_size
    merged_top, merged_total, merged_values = combined_by_axis(
        (
            local_top.reshape(row_count, head_cols),
            local_total.reshape(row_count, head_cols),
            local_values.reshape(row_count, head_cols * HD),
        ),
        KV,
        combine_parts,
    )
    own_score = jnp.einsum(
        "skgd,skd->skg",
        query_heads,
        new_key.reshape(row_count, local_heads, HD),
        preferred_element_type=jnp.float32,
    ).reshape(row_count, head_cols) * HD ** (-0.5)
    final_top = jnp.maximum(merged_top, own_score)
    past_scale = jnp.exp(merged_top - final_top)
    own_weight = jnp.exp(own_score - final_top)
    totals = merged_total * past_scale + own_weight
    own_rounded = lax.optimization_barrier(own_weight.astype(jnp.bfloat16)).astype(jnp.float32)
    own_values = jnp.broadcast_to(
        new_value.astype(jnp.float32).reshape(row_count, local_heads, 1, HD),
        (row_count, local_heads, group_size, HD),
    ).reshape(row_count, head_cols * HD)
    weighted = (
        merged_values * jnp.repeat(past_scale, HD, axis=1)
        + jnp.repeat(own_rounded, HD, axis=1) * own_values
    )
    attended = (weighted / jnp.repeat(totals, HD, axis=1)).astype(jnp.bfloat16)
    partial_out = jnp.dot(attended, out_weight, preferred_element_type=jnp.float32)
    head_sum = over_pieces(partial_out.astype(jnp.bfloat16), "tp").astype(jnp.float32)
    mid_cols = (token_rows + head_sum).astype(jnp.bfloat16)
    mid_rows = gathered_copies(mid_cols, KV, 1)
    mid_wide = mid_rows.astype(jnp.float32)
    normed_mid = (
        mid_wide
        * mlp_gain[None, :]
        * lax.rsqrt(jnp.mean(mid_wide * mid_wide, axis=1, keepdims=True) + epsilon)
    ).astype(jnp.bfloat16)
    hidden = jnp.square(
        jax.nn.relu(jnp.dot(normed_mid, up_weight, preferred_element_type=jnp.float32))
    ).astype(jnp.bfloat16)
    mixer_term = jnp.dot(hidden, down_weight, preferred_element_type=jnp.float32)
    kv_count = lax.axis_size(KV)
    tp_count = lax.axis_size("tp")
    block_cols = mixer_term.shape[1] // (kv_count * tp_count)
    reordered = (
        mixer_term.reshape(row_count, kv_count, tp_count, block_cols)
        .transpose(0, 2, 1, 3)
        .reshape(row_count, kv_count * tp_count * block_cols)
    )
    pair_share = sent_and_summed(reordered.astype(jnp.bfloat16), "tp", 1)
    mixer_share = sum_at_owner(pair_share, KV, 1)
    out_cols = mixer_share.shape[1]
    start_col = (kv_place * tp_count + tp_place) * out_cols
    mid_share = lax.dynamic_slice_in_dim(mid_wide, start_col, out_cols, 1)
    return (mid_share + mixer_share).astype(jnp.bfloat16)


def solution(mesh):
    torus = Mesh(
        mesh.devices.reshape(mesh.shape["dp"], 8, 8, mesh.shape["tp"]), ("dp", "kv_0", "kv_1", "tp")
    )
    placed = (
        P("dp", KV),
        P("dp"),
        P(KV),
        P(KV, "tp"),
        P(KV, "tp"),
        P(KV, "tp"),
        P(),
        P("tp"),
        P("dp", KV, "tp"),
        P("dp", KV, "tp"),
        P("dp", "tp", KV),
        P("tp", KV),
        P(),
        P(None, KV_TP),
        P(KV_TP, None),
    )
    return jax.shard_map(
        shards, mesh=torus, in_specs=placed, out_specs=P("dp", KV_TP), check_vma=False
    )
```

profile of v0, /device:TPU:1, one launch (start us, length us, event | category | flops | bytes accessed | tf_op | source)
XLA Modules:
  0.0 180.9 jit_solution(4492494843078950118)
XLA Ops:
  0.0 0.9 fusion.53
  0.9 0.9 convolution_convert_fusion.5
  1.8 0.9 convolution_convert_fusion.4
  2.7 1.1 convolution_convert_fusion.1
  3.8 0.9 convolution_convert_fusion.6
  4.7 30.1 %all-reduce.5 = (bf16[6,2048]{1,0:T(8,128)(2,1)S(1)}, bf16[6]{0:T(256)(128)(2,1)S(1)}, bf16[6,128]{1,0:T(8,128)(2,1)S(1)}, bf16[6,2]{0,1:T(2,128)(2,1)S(1)}, bf16[6,128]{1,0:T(8,128)(2,1)S(1)}) all-reduce(bf16[6,2048]{1,0:T(8,128)(2,1)S(1)} %convolution_convert_fusion.1, ...), channel_id=1, replica_groups=mesh['dp'=4,'kv_0'=8,'kv_1'=8,'tp'=2] {'kv_0'}, use_global_device_ids=true, to_apply=%region_0.0 | all-reduce | flops 13842 | bytes 55368 | tf_op jit(solution)/shard_map/psum | solution.py:22
  34.8 23.5 %all-reduce.4 = (bf16[6,2048]{1,0:T(8,128)(2,1)S(1)}, bf16[6]{0:T(256)(128)(2,1)S(1)}, bf16[6,128]{1,0:T(8,128)(2,1)S(1)}, bf16[6,2]{0,1:T(2,128)(2,1)S(1)}, bf16[6,128]{1,0:T(8,128)(2,1)S(1)}) all-reduce(bf16[6,2048]{1,0:T(8,128)(2,1)S(1)} %get-tuple-element.34, ...), channel_id=1, replica_groups=mesh['dp'=4,'kv_0'=8,'kv_1'=8,'tp'=2] {'kv_1'}, use_global_device_ids=true, to_apply=%region_1.0 | all-reduce | flops 13842 | bytes 55368 | tf_op jit(solution)/shard_map/psum | solution.py:22
  58.4 0.7 copy-done.8
  59.1 0.1 copy.47
  59.2 0.1 reshape.411
  59.4 0.2 copy.46
  59.6 0.4 copy-done.9
  60.1 0.3 select_reduce_fusion
  60.4 0.2 fusion.6
  60.7 0.1 convert_element_type.506
  60.8 0.3 copy-done.3
  61.1 0.2 copy.48
  61.3 0.3 convolution_convert_fusion.2
  61.5 0.1 convert_element_type.504
  61.7 18.7 %all-gather = bf16[64,2048]{1,0:T(8,128)(2,1)S(1)} all-gather(bf16[8,2048]{1,0:T(8,128)(2,1)S(1)} %pad_maximum_fusion), channel_id=2, replica_groups=mesh['dp'=4,'kv_0'=8,'kv_1'=8,'tp'=2] {'kv_0'}, dimensions={0}, use_global_device_ids=true | all-gather | bytes 294912 | tf_op jit(solution)/shard_map/all_gather | solution.py:33
  80.4 0.1 fusion.92
  80.9 0.1 fusion.93
  81.1 0.1 reshape.452
  82.1 0.1 reshape.429
  82.5 0.1 reshape.419
  82.7 0.1 reshape.417
  83.2 0.1 reshape.428
  83.4 0.1 reshape.426
  83.9 0.1 reshape.422
  84.1 0.1 reshape.420
  84.5 0.1 reshape.418
  84.7 18.4 %all-gather.1 = bf16[64,2048]{1,0:T(8,128)(2,1)S(1)} all-gather(bf16[8,2048]{1,0:T(8,128)(2,1)S(1)} %pad_maximum_fusion.1), channel_id=3, replica_groups=mesh['dp'=4,'kv_0'=8,'kv_1'=8,'tp'=2] {'kv_1'}, dimensions={0}, use_global_device_ids=true | all-gather | bytes 294912 | tf_op jit(solution)/shard_map/all_gather | solution.py:33
  103.1 0.1 fusion.91
  105.0 0.1 reshape.451
  105.3 0.1 reshape.436
  105.5 0.1 reshape.437
  105.7 0.1 reshape.438
  106.1 0.1 reshape.440
  106.2 0.1 reshape.441
  106.8 0.1 reshape.444
  107.0 0.1 reshape.445
  107.5 0.1 reshape.448
  107.8 0.6 copy-done.4
  108.4 0.2 fusion.4
  108.6 29.0 %all-gather.3 = bf16[2,6,64]{2,1,0:T(8,128)(2,1)S(1)} all-gather(bf16[1,6,64]{2,1,0:T(8,128)(2,1)S(1)} %fusion.4), channel_id=4, replica_groups=mesh['dp'=4,'kv_0'=8,'kv_1'=8,'tp'=2] {'tp'}, dimensions={0}, use_global_device_ids=true | all-gather | bytes 2304 | tf_op jit(solution)/shard_map/all_gather | solution.py:61
  137.7 0.1 reshape.648
  137.8 16.9 %all_to_all.15 = bf16[64,2,192]{2,1,0:T(2,128)(2,1)S(1)} all-to-all(bf16[64,2,192]{2,1,0:T(2,128)(2,1)S(1)} %reshape.648), channel_id=1, replica_groups=mesh['dp'=4,'kv_0'=8,'kv_1'=8,'tp'=2] {'kv_0','kv_1'}, dimensions={0} | all-to-all | bytes 98304 | tf_op jit(solution)/shard_map/all_to_all | solution.py:67
  154.8 0.1 reshape.649
  154.9 0.2 fusion.5
  155.2 0.1 reshape.513
  155.3 0.6 copy-done.6
  155.9 0.5 convolution_convert_fusion
  156.4 0.2 convert_element_type.643
  156.6 0.2 convert_element_type.645
  156.9 5.2 %all_to_all.16 = bf16[2,6,2048]{2,1,0:T(8,128)(2,1)S(1)} all-to-all(bf16[2,6,2048]{2,1,0:T(8,128)(2,1)S(1)} %copy.53), channel_id=1, replica_groups=mesh['dp'=4,'kv_0'=8,'kv_1'=8,'tp'=2] {'tp'}, dimensions={0} | all-to-all | bytes 98304 | tf_op jit(solution)/shard_map/all_to_all | solution.py:89
  162.1 0.1 reshape.455
  162.2 0.1 copy.54
  162.3 0.8 reshape.650
  163.1 4.6 %all-to-all-start.2 = ((f32[64,1,192]{2,1,0:T(1,128)}), f32[64,1,192]{2,1,0:T(1,128)S(1)}, u32[]{:S(2)}, u32[]{:S(2)}) async-start(f32[64,1,192]{2,1,0:T(1,128)} %reshape.650), calls=%async_computation.2 | async-start | bytes 131072 | tf_op jit(solution)/shard_map/all_to_all | solution.py:95
  167.7 11.1 %all-to-all-done.2 = f32[64,1,192]{2,1,0:T(1,128)S(1)} async-done(((f32[64,1,192]{2,1,0:T(1,128)}), f32[64,1,192]{2,1,0:T(1,128)S(1)}, u32[]{:S(2)}, u32[]{:S(2)}) %all-to-all-start.2) | async-done | bytes 49184 | tf_op jit(solution)/shard_map/all_to_all | solution.py:95
  178.8 0.5 broadcast.137
  179.3 0.8 reduce.99
  180.1 0.1 reshape.651
  180.3 0.7 add_convert_fusion
  (134 shorter events, 7.1 us)
Async XLA Ops:
  0.0 155.3 %copy-start = (bf16[128,4096]{1,0:T(8,128)(2,1)S(1)}, bf16[128,4096]{1,0:T(8,128)(2,1)}, u32[]{:S(2)}) copy-start(bf16[128,4096]{1,0:T(8,128)(2,1)} %param.29) | copy-start | bytes 3145732
  0.0 59.3 %copy-start.2 = (bf16[6,256,128]{2,1,0:T(8,128)(2,1)S(1)}, bf16[6,256,128]{2,1,0:T(8,128)(2,1)}, u32[]{:S(2)}) copy-start(bf16[6,256,128]{2,1,0:T(8,128)(2,1)} %param.23) | copy-start | bytes 1179652
  58.4 0.7 copy-start.8
  59.3 0.7 copy-start.9
  59.4 0.7 copy-start.7
  60.1 1.0 copy-start.3
  107.4 1.0 copy-start.4
  108.4 29.3 %copy-start.5 = (bf16[6,64]{1,0:T(8,128)(2,1)S(1)}, bf16[6,64]{1,0:T(8,128)(2,1)}, u32[]{:S(2)}) copy-start(bf16[6,64]{1,0:T(8,128)(2,1)} %param.15) | copy-start | bytes 2308
  108.6 46.7 %copy-start.1 = (bf16[4096,128]{1,0:T(8,128)(2,1)S(1)}, bf16[4096,128]{1,0:T(8,128)(2,1)}, u32[]{:S(2)}) copy-start(bf16[4096,128]{1,0:T(8,128)(2,1)} %param.28) | copy-start | bytes 3145732
  155.2 0.7 copy-start.6
  163.1 15.7 %all-to-all-start.2 = ((f32[64,1,192]{2,1,0:T(1,128)}), f32[64,1,192]{2,1,0:T(1,128)S(1)}, u32[]{:S(2)}, u32[]{:S(2)}) async-start(f32[64,1,192]{2,1,0:T(1,128)} %reshape.650), calls=%async_computation.2 | async-start | bytes 131072 | tf_op jit(solution)/shard_map/all_to_all | solution.py:95
where the time goes:
time: 182 us; the launch traced here: 181 us
  blocking collectives  142 us (78%)
  local copies, waits for them, and re-layouts  13.8 us (8%)
  waiting for transfers between devices  11.1 us (6%)
  matrix products  5.18 us (3%)
  starting transfers between devices  4.61 us (3%)
  other arithmetic  3.62 us (2%)
    psum x2, blocking collectives, over_axes(): return functools.reduce(lax.psum, axes, x)  53.6 us
    all_gather x2, blocking collectives, gathered_once(): both, at, found = (lax.all_gather(jnp.concatenate(lines), axis), 0, {})  37.2 us
    all_gather x1, blocking collectives, over_pieces(): pieces = lax.all_gather(x, axis).astype(jnp.float32)  29 us
    all_to_all x1, blocking collectives, from_everyone(): return lax.all_to_all(copies, axis, split_axis=0, concat_axis=0, tiled=True)  16.9 us
    all_to_all x1, waiting for transfers between devices, sum_at_owner(): lax.all_to_all(pieces, axis, split_axis=0, concat_axis=0, tiled=True)  11.1 us
    all_to_all x1, blocking collectives, sent_and_summed(): pieces = lax.all_to_all(cut_along(x, dim, devices), axis, 0, 0, tiled=True)  5.19 us
    all_to_all x1, starting transfers between devices, sum_at_owner(): lax.all_to_all(pieces, axis, split_axis=0, concat_axis=0, tiled=True)  4.61 us
    unnamed x29, local copies, waits for them, and re-layouts  4.17 us
  transfers between devices with their start and end apart: 1, of which 1 were waited for; matrix products, arithmetic and copies ran while one was open for 0% of the time, Pallas kernels for 0%

commit v1 on v0

--- a/solution.py
+++ b/solution.py
@@ -18,45 +18,6 @@
 floor_score = -1e30
 
 
-def over_axes(x, axes):
-    return functools.reduce(lax.psum, axes, x)
-
-
-def gathered_once(x, axis):
-    leaves = jax.tree.leaves(x)
-    order = sorted(range(len(leaves)), key=lambda k: -leaves[k].size)
-    width = (1, *leaves[order[0]].shape)[-1]
-    lines = [
-        jnp.pad(leaves[k].reshape(-1), (0, -leaves[k].size % width)).reshape(-1, width)
-        for k in order
-    ]
-    both, at, found = (lax.all_gather(jnp.concatenate(lines), axis), 0, {})
-    for k, line in zip(order, lines):
-        section = both[:, at : at + len(line)].reshape(len(both), -1)
-        found[k] = section[:, : leaves[k].size].reshape(-1, *leaves[k].shape)
-        at += len(line)
-    numbers = iter(range(len(leaves)))
-    return jax.tree.map(lambda _: found[next(numbers)], x)
-
-
-def combined_by_axis(x, axes, combine):
-    for axis in axes:
-        pieces = gathered_once(
-            jax.tree.map(
-                lambda part, kind: part.astype(kind), x, (jnp.bfloat16, jnp.bfloat16, jnp.bfloat16)
-            ),
-            axis,
-        )
-        widened = [
-            jax.tree.map(lambda part, own: part[k].astype(own.dtype), pieces, x)
-            for k in range(lax.axis_size(axis))
-        ]
-        x = widened[0]
-        for theirs in widened[1:]:
-            x = combine(x, theirs)
-    return x
-
-
 def over_pieces(x, axis):
     pieces = lax.all_gather(x, axis).astype(jnp.float32)
     return pieces.sum(axis=0)
@@ -90,25 +51,27 @@
     return jnp.sum(pieces.astype(jnp.float32), axis=0)
 
 
-def sum_at_owner(x, axis, dim):
-    pieces = cut_along(x, dim, lax.axis_size(axis))
-    arrived = lax.all_to_all(pieces, axis, split_axis=0, concat_axis=0, tiled=True)
-    return arrived.sum(axis=0)
-
-
-def combine_parts(earlier, later):
-    first_top, first_total, first_values = earlier
-    second_top, second_total, second_values = later
-    merged_top = jnp.maximum(first_top, second_top)
-    first_scale = jnp.exp(first_top - merged_top)
-    second_scale = jnp.exp(second_top - merged_top)
-    first_wide = jnp.repeat(first_scale, HD, axis=1)
-    second_wide = jnp.repeat(second_scale, HD, axis=1)
-    return (
-        merged_top,
-        first_total * first_scale + second_total * second_scale,
-        first_values * first_wide + second_values * second_wide,
-    )
+def summed_everywhere(x):
+    for axis in ("kv_1", "kv_0"):
+        x = from_everyone(x.astype(jnp.bfloat16), axis).astype(jnp.float32).sum(axis=0)
+    return x
+
+
+def combined_everywhere(top, total, values):
+    rows, heads = top.shape
+    for axis in ("kv_1", "kv_0"):
+        line = jnp.concatenate((values, top, total), axis=1).astype(jnp.bfloat16)
+        pieces = from_everyone(line, axis).astype(jnp.float32)
+        values = pieces[:, :, : heads * HD]
+        top = pieces[:, :, heads * HD : heads * (HD + 1)]
+        total = pieces[:, :, heads * (HD + 1) :]
+        merged = top.max(axis=0)
+        scale = jnp.exp(top - merged[None])
+        total = (total * scale).sum(axis=0)
+        wide = jnp.repeat(scale, HD, axis=2)
+        values = (values * wide).sum(axis=0)
+        top = merged
+    return top, total, values
 
 
 def shards(
@@ -146,13 +109,16 @@
         (feature_cols, local_heads),
     )
     forget_part = jnp.dot(scaled_rows, gate_rows, preferred_element_type=jnp.float32)
-    query_sum, key_sum, value_sum, forget_sum, square_sum = (
-        over_axes(query_part.astype(jnp.bfloat16), KV).astype(jnp.float32),
-        over_axes(key_part.astype(jnp.bfloat16), KV).astype(jnp.float32),
-        over_axes(value_part.astype(jnp.bfloat16), KV).astype(jnp.float32),
-        over_axes(forget_part.astype(jnp.bfloat16), KV).astype(jnp.float32),
-        over_axes(square_part.astype(jnp.bfloat16), KV).astype(jnp.float32),
-    )
+    widths = (query_part.shape[1], key_part.shape[1], value_part.shape[1], forget_part.shape[1])
+    parts = jnp.concatenate(
+        (query_part, key_part, value_part, forget_part, square_part[:, None]), axis=1
+    )
+    sums = summed_everywhere(parts)
+    query_sum = sums[:, : widths[0]]
+    key_sum = sums[:, widths[0] : widths[0] + widths[1]]
+    value_sum = sums[:, widths[0] + widths[1] : sum(widths[:3])]
+    forget_sum = sums[:, sum(widths[:3]) : sum(widths)]
+    square_sum = sums[:, sum(widths)]
     row_scale = lax.rsqrt(square_sum / D + epsilon)[:, None]
     queries = (query_sum * row_scale).astype(jnp.bfloat16)
     new_key = (key_sum * row_scale).astype(jnp.bfloat16)
@@ -169,6 +135,7 @@
     cache_pos = kv_place * positions_here + jnp.arange(positions_here)
     active_mask = (cache_pos[None, :] < lengths[:, None])[:, None, None, :]
     local_top = jnp.max(jnp.where(active_mask, scores, floor_score), axis=3)
+    local_top = local_top.astype(jnp.bfloat16).astype(jnp.float32)
     weights = jnp.where(active_mask, jnp.exp(scores - local_top[..., None]), 0.0)
     local_total = jnp.sum(weights, axis=3)
     local_values = jnp.einsum(
@@ -178,14 +145,10 @@
         preferred_element_type=jnp.float32,
     )
     head_cols = local_heads * group_size
-    merged_top, merged_total, merged_values = combined_by_axis(
-        (
-            local_top.reshape(row_count, head_cols),
-            local_total.reshape(row_count, head_cols),
-            local_values.reshape(row_count, head_cols * HD),
-        ),
-        KV,
-        combine_parts,
+    merged_top, merged_total, merged_values = combined_everywhere(
+        local_top.reshape(row_count, head_cols),
+        local_total.reshape(row_count, head_cols),
+        local_values.reshape(row_count, head_cols * HD),
     )
     own_score = jnp.einsum(
         "skgd,skd->skg",
@@ -223,14 +186,10 @@
     mixer_term = jnp.dot(hidden, down_weight, preferred_element_type=jnp.float32)
     kv_count = lax.axis_size(KV)
     tp_count = lax.axis_size("tp")
-    block_cols = mixer_term.shape[1] // (kv_count * tp_count)
-    reordered = (
-        mixer_term.reshape(row_count, kv_count, tp_count, block_cols)
-        .transpose(0, 2, 1, 3)
-        .reshape(row_count, kv_count * tp_count * block_cols)
-    )
-    pair_share = sent_and_summed(reordered.astype(jnp.bfloat16), "tp", 1)
-    mixer_share = sum_at_owner(pair_share, KV, 1)
+    pair_sum = over_pieces(mixer_term.astype(jnp.bfloat16), "tp")
+    pair_cols = sent_and_summed(pair_sum.astype(jnp.bfloat16), KV, 1)
+    out_width = pair_cols.shape[1] // tp_count
+    mixer_share = lax.dynamic_slice_in_dim(pair_cols, tp_place * out_width, out_width, 1)
     out_cols = mixer_share.shape[1]
     start_col = (kv_place * tp_count + tp_place) * out_cols
     mid_share = lax.dynamic_slice_in_dim(mid_wide, start_col, out_cols, 1)

time: 182 us -> 123 us (0.68)
  blocking collectives: 142 us -> 42.2 us
  waiting for transfers between devices: 11.1 us -> 37.8 us
  starting transfers between devices: 4.61 us -> 23.5 us
    psum x2 -> x0, blocking collectives: 53.6 us -> none  [over_axes(): return functools.reduce(lax.psum, axes, x)]
    all_gather x2 -> x0, blocking collectives: 37.2 us -> none  [gathered_once(): both, at, found = (lax.all_gather(jnp.concatenate(lines), axis), 0, {})]
    all_to_all x1 -> x4, waiting for transfers between devices: 11.1 us -> 37.8 us  [the longest x3 26.7 us: from_everyone(): return lax.all_to_all(copies, axis, split_axis=0, concat_axis=0, tiled=True)]
    all_gather x1 -> x2, blocking collectives: 29 us -> 9.31 us  [over_pieces(): pieces = lax.all_gather(x, axis).astype(jnp.float32)]
    all_to_all x1 -> x4, starting transfers between devices: 4.61 us -> 23.5 us  [the longest x3 18.9 us: from_everyone(): return lax.all_to_all(copies, axis, split_axis=0, concat_axis=0, tiled=True)]
    all_to_all x1 -> x2, blocking collectives: 16.9 us -> 32.9 us  [from_everyone(): return lax.all_to_all(copies, axis, split_axis=0, concat_axis=0, tiled=True)]
    all_to_all x1 -> x0, blocking collectives: 5.19 us -> none  [sent_and_summed(): pieces = lax.all_to_all(cut_along(x, dim, devices), axis, 0, 0, tiled=True)]
    convert_element_type x30 -> x1, local copies, waits for them, and re-layouts: 2.55 us -> 0.09 us  [shards(): local_top = local_top.astype(jnp.bfloat16).astype(jnp.float32)]
  transfers between devices with their start and end apart: 1 -> 4, of which waited for: 1 -> 4; matrix products, arithmetic and copies ran while one was open for 0% -> 1% of each run, Pallas kernels for 0% -> 0%
where the time goes in v1:
time: 123 us; the launch traced here: 122 us
  blocking collectives  42.2 us (34%)
  waiting for transfers between devices  37.8 us (31%)
  starting transfers between devices  23.5 us (19%)
  local copies, waits for them, and re-layouts  12 us (10%)
  matrix products  3.57 us (3%)
  other arithmetic  2.61 us (2%)
    all_to_all x2, blocking collectives, from_everyone(): return lax.all_to_all(copies, axis, split_axis=0, concat_axis=0, tiled=True)  32.9 us
    all_to_all x3, waiting for transfers between devices, from_everyone(): return lax.all_to_all(copies, axis, split_axis=0, concat_axis=0, tiled=True)  26.7 us
    all_to_all x3, starting transfers between devices, from_everyone(): return lax.all_to_all(copies, axis, split_axis=0, concat_axis=0, tiled=True)  18.9 us
    all_to_all x1, waiting for transfers between devices, sent_and_summed(): pieces = lax.all_to_all(cut_along(x, dim, devices), axis, 0, 0, tiled=True)  11.1 us
    all_gather x2, blocking collectives, over_pieces(): pieces = lax.all_gather(x, axis).astype(jnp.float32)  9.31 us
    unnamed x32, local copies, waits for them, and re-layouts  6.57 us
    all_to_all x1, starting transfers between devices, sent_and_summed(): pieces = lax.all_to_all(cut_along(x, dim, devices), axis, 0, 0, tiled=True)  4.61 us
  transfers between devices with their start and end apart: 4, of which 4 were waited for; matrix products, arithmetic and copies ran while one was open for 1% of the time, Pallas kernels for 0%

profile of v1, /device:TPU:1, one launch (start us, length us, event | category | flops | bytes accessed | tf_op | source)
XLA Modules:
  0.0 122.0 jit_solution(2104045043270476003)
XLA Ops:
  0.0 0.8 copy-done.5
  0.8 0.1 fusion.25
  0.9 0.7 copy-done.10
  1.5 0.9 convolution_convert_fusion.6
  2.4 0.1 copy.76
  2.5 1.1 convolution_convert_fusion.1
  3.6 0.1 copy.77
  3.8 0.1 convolution_convert_fusion.4
  3.9 0.5 copy-done.8
  4.4 0.1 convolution_convert_fusion.5
  4.5 0.1 concatenate.12
  4.6 18.0 %all_to_all.30 = bf16[8,6,2307]{2,1,0:T(8,128)(2,1)S(1)} all-to-all(bf16[8,6,2307]{2,1,0:T(8,128)(2,1)S(1)} %broadcast_in_dim.77), channel_id=1, replica_groups=mesh['dp'=4,'kv_0'=8,'kv_1'=8,'tp'=2] {'kv_1'}, dimensions={0} | all-to-all | bytes 442944 | tf_op jit(solution)/shard_map/all_to_all | solution.py:28
  22.7 0.7 broadcast_in_dim.78
  23.4 10.9 %all-to-all-start.1 = ((bf16[8,6,2307]{2,1,0:T(8,128)(2,1)}), bf16[8,6,2307]{2,1,0:T(8,128)(2,1)S(1)}, u32[]{:S(2)}, u32[]{:S(2)}) async-start(bf16[8,6,2307]{2,1,0:T(8,128)(2,1)} %broadcast_in_dim.78), calls=%async_computation.1 | async-start | bytes 622592 | tf_op jit(solution)/shard_map/all_to_all | solution.py:28
  34.4 0.2 copy.80
  34.6 0.8 copy-done.3
  35.4 0.2 copy.81
  35.6 0.6 copy-done.11
  36.3 8.1 %all-to-all-done.1 = bf16[8,6,2307]{2,1,0:T(8,128)(2,1)S(1)} async-done(((bf16[8,6,2307]{2,1,0:T(8,128)(2,1)}), bf16[8,6,2307]{2,1,0:T(8,128)(2,1)S(1)}, u32[]{:S(2)}, u32[]{:S(2)}) %all-to-all-start.1) | async-done | bytes 221504 | tf_op jit(solution)/shard_map/all_to_all | solution.py:28
  44.4 0.2 convert_reduce_fusion
  44.6 0.2 fusion.34
  44.8 0.1 reshape.100
  44.9 0.6 copy-done.12
  45.6 0.3 select_reduce_fusion
  45.9 0.2 fusion.9
  46.2 0.3 convolution_convert_fusion.2
  46.5 0.1 reshape.103
  46.6 0.1 concatenate.13
  46.7 0.7 broadcast_in_dim.81
  47.5 4.4 %all-to-all-start.2 = ((bf16[8,6,2112]{2,1,0:T(8,128)(2,1)}), bf16[8,6,2112]{2,1,0:T(8,128)(2,1)S(1)}, u32[]{:S(2)}, u32[]{:S(2)}) async-start(bf16[8,6,2112]{2,1,0:T(8,128)(2,1)} %broadcast_in_dim.81), calls=%async_computation.2 | async-start | bytes 557056 | tf_op jit(solution)/shard_map/all_to_all | solution.py:28
  52.0 9.4 %all-to-all-done.2 = bf16[8,6,2112]{2,1,0:T(8,128)(2,1)S(1)} async-done(((bf16[8,6,2112]{2,1,0:T(8,128)(2,1)}), bf16[8,6,2112]{2,1,0:T(8,128)(2,1)S(1)}, u32[]{:S(2)}, u32[]{:S(2)}) %all-to-all-start.2) | async-done | bytes 202784 | tf_op jit(solution)/shard_map/all_to_all | solution.py:28
  61.4 0.1 fusion.21
  61.5 0.3 broadcast_in_dim.82
  61.8 0.3 reshape.105
  62.1 0.2 fusion.7
  62.3 0.1 concatenate.14
  62.3 0.7 broadcast_in_dim.83
  63.1 3.7 %all-to-all-start.3 = ((bf16[8,6,2112]{2,1,0:T(8,128)(2,1)}), bf16[8,6,2112]{2,1,0:T(8,128)(2,1)S(1)}, u32[]{:S(2)}, u32[]{:S(2)}) async-start(bf16[8,6,2112]{2,1,0:T(8,128)(2,1)} %broadcast_in_dim.83), calls=%async_computation.3 | async-start | bytes 557056 | tf_op jit(solution)/shard_map/all_to_all | solution.py:28
  66.7 0.1 fusion.46
  67.0 0.1 reshape.110
  67.1 9.2 %all-to-all-done.3 = bf16[8,6,2112]{2,1,0:T(8,128)(2,1)S(1)} async-done(((bf16[8,6,2112]{2,1,0:T(8,128)(2,1)}), bf16[8,6,2112]{2,1,0:T(8,128)(2,1)S(1)}, u32[]{:S(2)}, u32[]{:S(2)}) %all-to-all-start.3) | async-done | bytes 202784 | tf_op jit(solution)/shard_map/all_to_all | solution.py:28
  76.5 0.3 broadcast_in_dim.84
  76.7 0.3 reshape.106
  77.0 0.1 fusion.6
  77.3 0.1 reshape.108
  77.5 0.1 reshape.109
  77.7 0.1 reshape.111
  77.8 0.6 copy-done.4
  78.3 0.2 fusion.5
  78.5 6.3 %all-gather.2 = bf16[2,6,64]{2,1,0:T(8,128)(2,1)S(1)} all-gather(bf16[1,6,64]{2,1,0:T(8,128)(2,1)S(1)} %fusion.5), channel_id=2, replica_groups=mesh['dp'=4,'kv_0'=8,'kv_1'=8,'tp'=2] {'tp'}, dimensions={0}, use_global_device_ids=true | all-gather | bytes 2304 | tf_op jit(solution)/shard_map/all_gather | solution.py:22
  84.8 0.1 reshape.130
  85.0 14.9 %all_to_all.31 = bf16[64,2,192]{2,1,0:T(2,128)(2,1)S(1)} all-to-all(bf16[64,2,192]{2,1,0:T(2,128)(2,1)S(1)} %reshape.130), channel_id=1, replica_groups=mesh['dp'=4,'kv_0'=8,'kv_1'=8,'tp'=2] {'kv_0','kv_1'}, dimensions={0} | all-to-all | bytes 98304 | tf_op jit(solution)/shard_map/all_to_all | solution.py:28
  99.8 0.1 reshape.131
  100.0 0.2 fusion.8
  100.2 0.1 reshape.114
  100.4 0.6 copy-done.6
  101.0 0.5 fusion
  101.5 3.0 %all-gather.3 = bf16[2,6,4096]{2,1,0:T(8,128)(2,1)S(1)} all-gather(bf16[1,6,4096]{2,1,0:T(8,128)(2,1)S(1)} %fusion), channel_id=3, replica_groups=mesh['dp'=4,'kv_0'=8,'kv_1'=8,'tp'=2] {'tp'}, dimensions={0}, use_global_device_ids=true | all-gather | bytes 147456 | tf_op jit(solution)/shard_map/all_gather | solution.py:22
  104.5 0.1 reshape.112
  104.7 0.7 reshape.132
  105.5 4.6 %all-to-all-start.5 = ((bf16[64,2,192]{2,1,0:T(2,128)(2,1)}), bf16[64,2,192]{2,1,0:T(2,128)(2,1)S(1)}, u32[]{:S(2)}, u32[]{:S(2)}) async-start(bf16[64,2,192]{2,1,0:T(2,128)(2,1)} %reshape.132), calls=%async_computation.5 | async-start | bytes 131072 | tf_op jit(solution)/shard_map/all_to_all | solution.py:50
  110.1 11.1 %all-to-all-done.5 = bf16[64,2,192]{2,1,0:T(2,128)(2,1)S(1)} async-done(((bf16[64,2,192]{2,1,0:T(2,128)(2,1)}), bf16[64,2,192]{2,1,0:T(2,128)(2,1)S(1)}, u32[]{:S(2)}, u32[]{:S(2)}) %all-to-all-start.5) | async-done | bytes 49184 | tf_op jit(solution)/shard_map/all_to_all | solution.py:50
  121.2 0.1 reshape.133
  121.4 0.7 add_convert_fusion
  (52 shorter events, 1.6 us)
Async XLA Ops:
  0.0 100.4 %copy-start = (bf16[128,4096]{1,0:T(8,128)(2,1)S(1)}, bf16[128,4096]{1,0:T(8,128)(2,1)}, u32[]{:S(2)}) copy-start(bf16[128,4096]{1,0:T(8,128)(2,1)} %param.29) | copy-start | bytes 3145732
  0.0 0.8 copy-start.5
  0.9 0.7 copy-start.10
  2.5 1.2 %copy-start.7 = (bf16[64,128]{1,0:T(8,128)(2,1)S(1)}, bf16[64,128]{1,0:T(8,128)(2,1)}, u32[]{:S(2)}) copy-start(bf16[64,128]{1,0:T(8,128)(2,1)} %param.20) | copy-start | bytes 49156
  3.6 0.7 copy-start.8
  23.4 10.9 %copy-start.2 = (bf16[6,256,128]{2,1,0:T(8,128)(2,1)S(1)}, bf16[6,256,128]{2,1,0:T(8,128)(2,1)}, u32[]{:S(2)}) copy-start(bf16[6,256,128]{2,1,0:T(8,128)(2,1)} %param.23) | copy-start | bytes 1179652
  23.4 20.9 %all-to-all-start.1 = ((bf16[8,6,2307]{2,1,0:T(8,128)(2,1)}), bf16[8,6,2307]{2,1,0:T(8,128)(2,1)S(1)}, u32[]{:S(2)}, u32[]{:S(2)}) async-start(bf16[8,6,2307]{2,1,0:T(8,128)(2,1)} %broadcast_in_dim.78), calls=%async_computation.1 | async-start | bytes 622592 | tf_op jit(solution)/shard_map/all_to_all | solution.py:28
  34.4 1.0 copy-start.3
  35.6 0.7 copy-start.11
  44.8 0.7 copy-start.12
  44.8 0.7 copy-start.9
  47.5 13.9 %all-to-all-start.2 = ((bf16[8,6,2112]{2,1,0:T(8,128)(2,1)}), bf16[8,6,2112]{2,1,0:T(8,128)(2,1)S(1)}, u32[]{:S(2)}, u32[]{:S(2)}) async-start(bf16[8,6,2112]{2,1,0:T(8,128)(2,1)} %broadcast_in_dim.81), calls=%async_computation.2 | async-start | bytes 557056 | tf_op jit(solution)/shard_map/all_to_all | solution.py:28
  63.1 13.3 %all-to-all-start.3 = ((bf16[8,6,2112]{2,1,0:T(8,128)(2,1)}), bf16[8,6,2112]{2,1,0:T(8,128)(2,1)S(1)}, u32[]{:S(2)}, u32[]{:S(2)}) async-start(bf16[8,6,2112]{2,1,0:T(8,128)(2,1)} %broadcast_in_dim.83), calls=%async_computation.3 | async-start | bytes 557056 | tf_op jit(solution)/shard_map/all_to_all | solution.py:28
  77.4 1.0 copy-start.4
  78.5 21.9 %copy-start.1 = (bf16[4096,128]{1,0:T(8,128)(2,1)S(1)}, bf16[4096,128]{1,0:T(8,128)(2,1)}, u32[]{:S(2)}) copy-start(bf16[4096,128]{1,0:T(8,128)(2,1)} %param.28) | copy-start | bytes 3145732
  100.2 0.7 copy-start.6
  105.5 15.7 %all-to-all-start.5 = ((bf16[64,2,192]{2,1,0:T(2,128)(2,1)}), bf16[64,2,192]{2,1,0:T(2,128)(2,1)S(1)}, u32[]{:S(2)}, u32[]{:S(2)}) async-start(bf16[64,2,192]{2,1,0:T(2,128)(2,1)} %reshape.132), calls=%async_computation.5 | async-start | bytes 131072 | tf_op jit(solution)/shard_map/all_to_all | solution.py:50

commit v2 on v1

v2 whole, which is shorter than its diff:
```python
import functools

import jax
import jax.numpy as jnp
from jax import lax
from jax.experimental import pallas as pl
from jax.experimental.pallas import tpu as pltpu
from jax.sharding import Mesh
from jax.sharding import PartitionSpec as P

D = 4096
HEADS = 64
HD = 64
KEY_VALUE_HEADS = 4
KV = ("kv_0", "kv_1")
KV_TP = ("kv_0", "kv_1", "tp")
LANES = 128
HALF = 64
RING = 8

epsilon = 1e-06
floor_score = -1e30

VMEM = pl.BlockSpec(memory_space=pltpu.VMEM)
SMEM = pl.BlockSpec(memory_space=pltpu.SMEM)


def call(body, out_shape, in_specs, scratch=(), flops=1 << 20):
    return pl.pallas_call(
        body,
        out_shape=out_shape,
        in_specs=in_specs,
        out_specs=jax.tree.map(lambda _: VMEM, out_shape),
        scratch_shapes=scratch,
        compiler_params=pltpu.CompilerParams(vmem_limit_bytes=16 << 20),
        cost_estimate=pl.CostEstimate(flops=flops, bytes_accessed=1 << 20, transcendentals=0),
    )


def lanes_of(shape):
    return lax.broadcasted_iota(jnp.int32, shape, len(shape) - 1)


def rounded(x):
    return x.astype(jnp.bfloat16).astype(jnp.float32)


def exchanged(x, axes):
    return lax.all_to_all(x, axes, split_axis=0, concat_axis=0, tiled=True)


def dotted(a, b, b_dim=0):
    return lax.dot_general(
        a, b, (((1,), (b_dim,)), ((), ())), preferred_element_type=jnp.float32
    )


def project(place, tokens, gain, query_w, key_w, value_w, forget_w, out):
    rows = tokens[...].astype(jnp.float32)
    scaled = (rows * gain[...]).astype(jnp.bfloat16)
    wide = scaled.astype(jnp.float32)
    gates = forget_w[...].astype(jnp.float32)
    square = jnp.sum(rows * rows, axis=1, keepdims=True)
    square_high = rounded(square)
    columns = [
        jnp.sum(wide * gates[n : n + 1, :], axis=1, keepdims=True) for n in range(gates.shape[0])
    ] + [square_high, square - square_high]
    lane = lanes_of((rows.shape[0], LANES))
    extra = jnp.zeros(lane.shape, jnp.float32)
    for n, column in enumerate(columns):
        extra = jnp.where(lane == n, column, extra)
    line = jnp.concatenate(
        (
            dotted(scaled, query_w[...]),
            dotted(scaled, key_w[...]),
            dotted(scaled, value_w[...]),
            extra,
        ),
        axis=1,
    ).astype(jnp.bfloat16)
    for k in range(RING):
        out[k] = line


def summed(parts):
    total = parts[0].astype(jnp.float32)
    for k in range(1, RING):
        total = total + parts[k].astype(jnp.float32)
    return total


def resend(parts, out):
    line = summed(parts).astype(jnp.bfloat16)
    for k in range(RING):
        out[k] = line


def attend(place, lengths, offsets, parts, keys, values, gate, out, turned):
    count, positions = keys.shape[0], keys.shape[1]
    pairs = turned.shape[0] // 8
    spot, core = place[0], place[1]
    line = summed(parts)
    width = pairs * LANES
    extra = line[:, width + 2 * LANES :]
    row_scale = lax.rsqrt((extra[:, 4:5] + extra[:, 5:6]) / D + epsilon)
    ready = rounded(line[:, : width + 2 * LANES] * row_scale)
    new_key = ready[:, width : width + LANES]
    new_value = ready[:, width + LANES :]
    forget = []
    for n in range(2):
        gate_in = jnp.where(core == 0, extra[:, n : n + 1], extra[:, n + 2 : n + 3])
        z = gate_in * row_scale + offsets[n]
        forget.append(jnp.minimum(z, 0.0) - jnp.log1p(jnp.exp(-jnp.abs(z))))
    for j in range(pairs):
        turned[8 * j : 8 * j + count, :] = ready[:, LANES * j : LANES * (j + 1)]
    lane = lanes_of((pairs, LANES))
    row = lax.broadcasted_iota(jnp.int32, (pairs, LANES), 0)
    straight = (lane < HALF) == (row < pairs // 2)
    first = spot == 0
    place_of = spot * positions + lanes_of((1, positions))
    stat_lane = lanes_of((8, LANES))
    stats = jnp.zeros((8, LANES), jnp.float32)
    blocks = []
    for s in range(count):
        both = turned[pl.ds(s, pairs, stride=8), :]
        query = jnp.concatenate(
            (
                jnp.where(straight, both, 0.0),
                jnp.where(straight, pltpu.roll(both, HALF, 1), 0.0),
            ),
            axis=0,
        )
        score = dotted(query.astype(jnp.bfloat16), keys[s], 1) * HD ** (-0.5)
        lines = [
            jnp.broadcast_to(gate[s, n : n + 1, :] + forget[n][s : s + 1, :], (8, positions))
            for n in range(2)
        ]
        live = place_of < lengths[s]
        score = jnp.where(live, score + jnp.concatenate(lines + lines, axis=0), floor_score)
        own = jnp.sum(query * new_key[s : s + 1, :], axis=1, keepdims=True) * HD ** (-0.5)
        own = jnp.where(first, own, floor_score)
        top = rounded(jnp.maximum(jnp.max(score, axis=1, keepdims=True), own))
        weight = jnp.where(live, jnp.exp(score - top), 0.0)
        own_weight = jnp.where(first, jnp.exp(own - top), 0.0)
        total = jnp.sum(weight, axis=1, keepdims=True) + own_weight
        mixed = dotted(weight.astype(jnp.bfloat16), values[s])
        mixed = mixed + rounded(own_weight) * new_value[s : s + 1, :]
        blocks.append(
            jnp.where(straight, mixed[:pairs], pltpu.roll(mixed[pairs:], HALF, 1)).astype(
                jnp.bfloat16
            )
        )
        total_high = rounded(total)
        for n, column in enumerate((top, total_high, total - total_high)):
            for g in range(4):
                stats = jnp.where(
                    stat_lane == 32 * g + 8 * n + s, column[8 * g : 8 * g + 8], stats
                )
    blocks.append(stats.astype(jnp.bfloat16))
    line = jnp.concatenate(blocks, axis=0)
    for k in range(RING):
        out[k] = line


def spread(compact, block, low):
    s, half = divmod(block, 2)
    left, right = (s, 64 + s) if half == 0 else (96 + s, 32 + s)
    return jnp.where(low, compact[:, left : left + 1], compact[:, right : right + 1])


def merged(parts):
    rows = parts.shape[1]
    blocks = rows // 8 - 1
    stats = [parts[k, rows - 8 : rows, :].astype(jnp.float32) for k in range(RING)]
    top = functools.reduce(jnp.maximum, stats)
    scales = [jnp.exp(x - top) for x in stats]
    total = functools.reduce(
        jnp.add,
        [
            scale * (pltpu.roll(x, LANES - 8, 1) + pltpu.roll(x, LANES - 16, 1))
            for scale, x in zip(scales, stats)
        ],
    )
    low = lanes_of((8, LANES)) < HALF
    mixed = []
    for b in range(blocks):
        acc = jnp.zeros((8, LANES), jnp.float32)
        for k in range(RING):
            acc = acc + parts[k, 8 * b : 8 * b + 8, :].astype(jnp.float32) * spread(
                scales[k], b, low
            )
        mixed.append(acc)
    return top, total, mixed, low


def combine(parts, out):
    top, total, mixed, _ = merged(parts)
    kind = lanes_of((8, LANES)) % 32
    total_high = rounded(total)
    stats = jnp.where(
        kind < 8,
        top,
        jnp.where(
            kind < 16, pltpu.roll(total_high, 8, 1), pltpu.roll(total - total_high, 16, 1)
        ),
    )
    line = jnp.concatenate([x.astype(jnp.bfloat16) for x in mixed + [stats]], axis=0)
    for k in range(RING):
        out[k] = line


def finish(place, parts, tokens, out_w, out, turned):
    _, total, mixed, low = merged(parts)
    inverse = 1.0 / total
    for b, acc in enumerate(mixed):
        turned[8 * b : 8 * b + 8, :] = rounded(acc * spread(inverse, b, low))
    count = tokens.shape[0]
    pairs = turned.shape[0] // count
    attended = jnp.concatenate(
        [turned[pl.ds(j, count, stride=pairs), :] for j in range(pairs)], axis=1
    ).astype(jnp.bfloat16)
    part = dotted(attended, out_w[...], 1)
    part = part + jnp.where(place[1] == 0, tokens[...].astype(jnp.float32), 0.0)
    third = count // 2
    piece = jnp.concatenate((part[:third], part[third:]), axis=1).astype(jnp.bfloat16)
    for k in range(out.shape[0]):
        out[k] = piece


def mix(parts, gain, up_w, down_w, mid_out, out, mid):
    count, width = mid.shape
    third = count // 2
    low = lanes_of((third, LANES)) < HALF
    square = jnp.zeros((count, LANES), jnp.float32)
    for t in range(width // LANES):
        a = rounded(
            parts[4 * t].astype(jnp.float32) + parts[4 * t + 1].astype(jnp.float32)
        )
        b = rounded(
            parts[4 * t + 2].astype(jnp.float32) + parts[4 * t + 3].astype(jnp.float32)
        )
        at = slice(LANES * t, LANES * (t + 1))
        mid[:third, at] = jnp.where(low, a, pltpu.roll(b, HALF, 1))
        mid[third:, at] = jnp.where(low, pltpu.roll(a, HALF, 1), b)
        tile = mid[:, at]
        square = square + tile * tile
    scale = lax.rsqrt(jnp.sum(square, axis=1, keepdims=True) / D + epsilon)
    rows = mid[...]
    mid_out[...] = rows.astype(jnp.bfloat16)
    normed = (rows * gain[...] * scale).astype(jnp.bfloat16)
    hidden = jnp.square(jnp.maximum(dotted(normed, up_w[...]), 0.0))
    hidden = jnp.concatenate((hidden, jnp.zeros((8 - count, LANES), jnp.float32)), axis=0)
    picked = jnp.concatenate(
        [
            hidden[4 * a + (u + k) % 4 : 4 * a + (u + k) % 4 + 1]
            for k in range(4)
            for u in range(4)
            for a in range(2)
        ],
        axis=0,
    ).astype(jnp.bfloat16)
    spread_out = dotted(picked, down_w[...])
    group = lanes_of((8, LANES)) // 32
    owner = lax.broadcasted_iota(jnp.int32, (8, LANES), 0) // 2
    turn = (group - owner) % 4
    for t in range(width // LANES):
        at = slice(LANES * t, LANES * (t + 1))
        tile = spread_out[:8, at]
        for k in range(1, 4):
            tile = jnp.where(
                turn == k, pltpu.roll(spread_out[8 * k : 8 * k + 8, at], 32 * k, 1), tile
            )
        out[8 * t : 8 * t + 8, :] = tile.astype(jnp.bfloat16)


def close(place, parts, mid, out):
    total = jnp.zeros((8, LANES), jnp.float32)
    for t in range(parts.shape[0] // 8):
        total = total + parts[8 * t : 8 * t + 8, :].astype(jnp.float32)
    pair = total[0:2] + total[2:4] + total[4:6] + total[6:8]
    count, width = out.shape
    number = place[0] * 2 + place[1]
    tile = mid[:, pl.ds(pl.multiple_of((number // 4) * LANES, LANES), LANES)]
    group = number % 4
    own = jnp.zeros((count, width), jnp.float32)
    for n in range(4):
        own = jnp.where(
            group == n, tile[:, width * n : width * (n + 1)].astype(jnp.float32), own
        )
    rows = [pair[r // 4 : r // 4 + 1, 32 * (r % 4) : 32 * (r % 4) + 32] for r in range(count)]
    out[...] = (own + jnp.concatenate(rows, axis=0)).astype(jnp.bfloat16)


def shards(
    tokens,
    lengths,
    attn_gain,
    query_weight,
    key_weight,
    value_weight,
    forget_weight,
    forget_offset,
    cache_keys,
    cache_values,
    gate_sum,
    out_weight,
    mlp_gain,
    up_weight,
    down_weight,
):
    rows, cols = tokens.shape
    spot = lax.axis_index(KV)
    place = jnp.stack((spot, lax.axis_index("tp"))).astype(jnp.int32)
    bf16 = functools.partial(jax.ShapeDtypeStruct, dtype=jnp.bfloat16)
    heads_wide = query_weight.shape[1]
    line = heads_wide + 3 * LANES
    gates = lax.dynamic_slice(
        forget_weight.T, (0, spot * cols), (forget_weight.shape[1], cols)
    )
    x = call(project, bf16((RING, rows, line)), [SMEM] + [VMEM] * 6)(
        place, tokens, attn_gain[None, :], query_weight, key_weight, value_weight, gates
    )
    x = exchanged(x, "kv_1")
    x = call(resend, bf16((RING, rows, line)), [VMEM])(x)
    x = exchanged(x, "kv_0")
    stack = rows * heads_wide // LANES
    packed = stack + 8
    x = call(
        attend,
        bf16((RING, packed, LANES)),
        [SMEM] * 3 + [VMEM] * 4,
        [pltpu.VMEM((8 * heads_wide // LANES, LANES), jnp.float32)],
    )(place, lengths, forget_offset, x, cache_keys, cache_values, gate_sum)
    x = exchanged(x, "kv_1")
    x = call(combine, bf16((RING, packed, LANES)), [VMEM])(x)
    x = exchanged(x, "kv_0")
    group = lax.axis_size(KV_TP)
    x = call(
        finish,
        bf16((group, rows // 2, LANES)),
        [SMEM] + [VMEM] * 3,
        [pltpu.VMEM((stack, LANES), jnp.float32)],
    )(place, x, tokens, out_weight.T)
    x = exchanged(x, KV_TP)
    mid, x = call(
        mix,
        (bf16((rows, D)), bf16((2 * group, LANES))),
        [VMEM] * 4,
        [pltpu.VMEM((rows, D), jnp.float32)],
    )(x, mlp_gain[None, :], up_weight, down_weight)
    x = exchanged(x.reshape(group, 2, LANES), KV_TP).reshape(2 * group, LANES)
    return call(close, bf16((rows, D // group)), [SMEM, VMEM, VMEM])(place, x, mid)


def solution(mesh):
    torus = Mesh(
        mesh.devices.reshape(mesh.shape["dp"], 8, 8, mesh.shape["tp"]), ("dp", "kv_0", "kv_1", "tp")
    )
    placed = (
        P("dp", KV),
        P("dp"),
        P(KV),
        P(KV, "tp"),
        P(KV, "tp"),
        P(KV, "tp"),
        P(),
        P("tp"),
        P("dp", KV, "tp"),
        P("dp", KV, "tp"),
        P("dp", "tp", KV),
        P("tp", KV),
        P(),
        P(None, KV_TP),
        P(KV_TP, None),
    )
    return jax.shard_map(
        shards, mesh=torus, in_specs=placed, out_specs=P("dp", KV_TP), check_vma=False
    )
```

time: 123 us -> 112 us (0.911)
  blocking collectives: 42.2 us -> 102 us
  waiting for transfers between devices: 37.8 us -> 0 us
  starting transfers between devices: 23.5 us -> 0 us
  local copies, waits for them, and re-layouts: 12 us -> 2.39 us
  Pallas kernels: 0 us -> 7.01 us
  matrix products: 3.57 us -> 0 us
  other arithmetic: 2.61 us -> 0.08 us
    all_to_all x2 -> x6, blocking collectives: 32.9 us -> 102 us  [exchanged(): return lax.all_to_all(x, axes, split_axis=0, concat_axis=0, tiled=True)]
    all_to_all x4 -> x0, waiting for transfers between devices: 37.8 us -> none  [the longest x3 26.7 us: from_everyone(): return lax.all_to_all(copies, axis, split_axis=0, concat_axis=0, tiled=True)]
    all_to_all x4 -> x0, starting transfers between devices: 23.5 us -> none  [the longest x3 18.9 us: from_everyone(): return lax.all_to_all(copies, axis, split_axis=0, concat_axis=0, tiled=True)]
    all_gather x2 -> x0, blocking collectives: 9.31 us -> none  [over_pieces(): pieces = lax.all_gather(x, axis).astype(jnp.float32)]
    pallas_call x0 -> x7, Pallas kernels: none -> 7.01 us  [the longest x1 2.38 us: shards(): call(attend, bf16((RING, packed, LANES)), [SMEM] * 3 + [VMEM] * 4, [pltpu...]
    unnamed x32 -> x30, local copies, waits for them, and re-layouts: 6.57 us -> 2.32 us
    dot_general x9 -> x0, matrix products: 3.57 us -> none  [the longest x1 1.11 us: shards(): jnp.dot(scaled_rows, query_weight, preferred_element_type=jnp.float32)]
    broadcast_in_dim x13 -> x0, local copies, waits for them, and re-layouts: 3.19 us -> none  [the longest x5 2.23 us: from_everyone(): copies = jnp.broadcast_to(x, (lax.axis_size(axis), *x.shape))]
  transfers between devices with their start and end apart: 4 -> 0, of which waited for: 4 -> 0; matrix products, arithmetic and copies ran while one was open for 1% -> 0% of each run, Pallas kernels for 0% -> 0%
where the time goes in v2:
time: 112 us
  blocking collectives  102 us (91%)
  Pallas kernels  7.01 us (6%)
  local copies, waits for them, and re-layouts  2.39 us (2%)
    all_to_all x6, blocking collectives, exchanged(): return lax.all_to_all(x, axes, split_axis=0, concat_axis=0, tiled=True)  102 us
    pallas_call x1, Pallas kernels, shards(): call(attend, bf16((RING, packed, LANES)), [SMEM] * 3 + [VMEM] * 4, [pltpu...  2.38 us
    unnamed x30, local copies, waits for them, and re-layouts  2.32 us

profile of v2, /device:TPU:1, one launch (start us, length us, event | category | flops | bytes accessed | tf_op | source)
XLA Modules:
  0.0 111.7 jit_solution(4979571804609585009)
XLA Ops:
  0.0 0.0 copy-start
  0.0 0.0 copy-start.11
  0.0 0.0 copy-start.8
  0.0 0.0 copy-start.9
  0.0 0.1 pad_add_fusion.place
  0.1 0.7 copy-done
  0.8 0.1 dynamic-slice_bitcast_fusion.forget_w
  0.8 0.0 copy-start.12
  0.8 0.0 copy-done.11
  0.8 0.0 copy-done.8
  0.8 0.0 copy-done.9
  0.8 0.6 copy-done.12
  1.5 0.0 copy-start.5
  1.5 0.9 copy-done.5
  2.4 0.7 shard_map.145
  3.1 18.0 %all_to_all.30.parts = bf16[8,6,2432]{2,1,0:T(8,128)(2,1)S(1)} all-to-all(bf16[8,6,2432]{2,1,0:T(8,128)(2,1)S(1)} %shard_map.145), channel_id=1, replica_groups=mesh['dp'=4,'kv_0'=8,'kv_1'=8,'tp'=2] {'kv_1'}, dimensions={0} | all-to-all | bytes 466944 | tf_op jit(solution)/shard_map/all_to_all | solution.py:49
  21.2 0.0 copy-start.4
  21.2 0.0 copy-start.3
  21.3 0.0 copy-start.10
  21.3 0.0 copy-start.13
  21.3 0.0 copy-start.14
  21.3 20.5 %all_to_all.31.parts = bf16[8,6,2432]{2,1,0:T(8,128)(2,1)S(1)} all-to-all(bf16[8,6,2432]{2,1,0:T(8,128)(2,1)S(1)} %shard_map.146), channel_id=1, replica_groups=mesh['dp'=4,'kv_0'=8,'kv_1'=8,'tp'=2] {'kv_0'}, dimensions={0} | all-to-all | bytes 466944 | tf_op jit(solution)/shard_map/all_to_all | solution.py:49
  41.8 0.0 copy-done.4
  41.8 0.0 copy-done.3
  41.8 0.0 copy-done.10
  41.8 0.0 copy-done.13
  41.8 0.0 copy-done.14
  41.8 0.0 copy-start.6
  41.8 2.4 %shard_map.147 = bf16[8,104,128]{2,1,0:T(8,128)(2,1)S(1)} custom-call(s32[2]{0:T(128)S(1)} %pad_add_fusion.place, s32[6]{0:T(128)S(1)} %copy-done.13, f32[2]{0:T(128)S(1)} %copy-done.14, bf16[8,6,2432]{2,1,0:T(8,128)(2,1)S(1)} %all_to_all.31.parts, bf16[6,256,128]{2,1,0:T(8,128)(2,1)S(1)} %copy-done.3, bf16[6,256,128]{2,1,0:T(8,128)(2,1)S(1)} %copy-done.4, ...), custom_call_target="tpu_custom_call" | custom-call | flops 1048576 | bytes 1048576 | tf_op jit(solution)/shard_map/pallas_call | solution.py:328
  44.2 0.0 copy-start.1
  44.2 0.0 copy-start.2
  44.2 13.1 %all_to_all.32.parts = bf16[8,104,128]{2,1,0:T(8,128)(2,1)S(1)} all-to-all(bf16[8,104,128]{2,1,0:T(8,128)(2,1)S(1)} %shard_map.147), channel_id=1, replica_groups=mesh['dp'=4,'kv_0'=8,'kv_1'=8,'tp'=2] {'kv_1'}, dimensions={0} | all-to-all | bytes 425984 | tf_op jit(solution)/shard_map/all_to_all | solution.py:49
  57.3 0.4 shard_map.148
  57.7 12.4 %all_to_all.33.parts = bf16[8,104,128]{2,1,0:T(8,128)(2,1)S(1)} all-to-all(bf16[8,104,128]{2,1,0:T(8,128)(2,1)S(1)} %shard_map.148), channel_id=1, replica_groups=mesh['dp'=4,'kv_0'=8,'kv_1'=8,'tp'=2] {'kv_0'}, dimensions={0} | all-to-all | bytes 425984 | tf_op jit(solution)/shard_map/all_to_all | solution.py:49
  70.2 0.0 copy-done.6
  70.2 1.3 %shard_map.149 = bf16[128,3,128]{2,1,0:T(4,128)(2,1)S(1)} custom-call(s32[2]{0:T(128)S(1)} %pad_add_fusion.place, bf16[8,104,128]{2,1,0:T(8,128)(2,1)S(1)} %all_to_all.33.parts, bf16[6,64]{1,0:T(8,128)(2,1)S(1)} %copy-done.11, bf16[64,2048]{1,0:T(8,128)(2,1)S(1)} %bitcast.9), custom_call_target="tpu_custom_call" | custom-call | flops 1048576 | bytes 1048576 | tf_op jit(solution)/shard_map/pallas_call | solution.py:338
  71.5 0.0 copy-start.7
  71.5 21.5 %all_to_all.34.parts = bf16[128,3,128]{2,1,0:T(4,128)(2,1)S(1)} all-to-all(bf16[128,3,128]{2,1,0:T(4,128)(2,1)S(1)} %shard_map.149), channel_id=1, replica_groups=mesh['dp'=4,'kv_0'=8,'kv_1'=8,'tp'=2] {'kv_0','kv_1','tp'}, dimensions={0} | all-to-all | bytes 196608 | tf_op jit(solution)/shard_map/all_to_all | solution.py:49
  93.0 0.0 copy-done.1
  93.0 0.0 copy-done.2
  93.0 0.0 copy-done.7
  93.0 0.8 shard_map.150
  93.8 16.5 %all_to_all.35 = bf16[128,2,128]{2,1,0:T(2,128)(2,1)S(1)} all-to-all(bf16[128,2,128]{2,1,0:T(2,128)(2,1)S(1)} %bitcast.11), channel_id=1, replica_groups=mesh['dp'=4,'kv_0'=8,'kv_1'=8,'tp'=2] {'kv_0','kv_1','tp'}, dimensions={0} | all-to-all | bytes 131072 | tf_op jit(solution)/shard_map/all_to_all | solution.py:49
  110.3 1.4 %shard_map.151 = bf16[6,32]{1,0:T(8,128)(2,1)} custom-call(s32[2]{0:T(128)S(1)} %pad_add_fusion.place, bf16[256,128]{1,0:T(8,128)(2,1)S(1)} %bitcast.10, bf16[6,4096]{1,0:T(8,128)(2,1)S(1)} %get-tuple-element.8.mid), custom_call_target="tpu_custom_call" | custom-call | flops 1048576 | bytes 1048576 | tf_op jit(solution)/shard_map/pallas_call | solution.py:352
  (1 shorter events, 0.0 us)
Async XLA Ops:
  0.0 0.8 copy-start
  0.0 0.8 copy-start.11
  0.0 0.8 copy-start.8
  0.0 0.8 copy-start.9
  0.8 0.7 copy-start.12
  1.5 0.9 copy-start.5
  21.2 20.6 %copy-start.4 = (bf16[6,256,128]{2,1,0:T(8,128)(2,1)S(1)}, bf16[6,256,128]{2,1,0:T(8,128)(2,1)}, u32[]{:S(2)}) copy-start(bf16[6,256,128]{2,1,0:T(8,128)(2,1)} %values.1) | copy-start | bytes 1179652
  21.2 20.6 %copy-start.3 = (bf16[6,256,128]{2,1,0:T(8,128)(2,1)S(1)}, bf16[6,256,128]{2,1,0:T(8,128)(2,1)}, u32[]{:S(2)}) copy-start(bf16[6,256,128]{2,1,0:T(8,128)(2,1)} %keys.1) | copy-start | bytes 1179652
  21.3 20.6 %copy-start.10 = (f32[6,2,256]{2,1,0:T(2,128)S(1)}, f32[6,2,256]{2,1,0:T(2,128)}, u32[]{:S(2)}) copy-start(f32[6,2,256]{2,1,0:T(2,128)} %gate.1) | copy-start | bytes 36868
  21.3 20.5 %copy-start.13 = (s32[6]{0:T(128)S(1)}, s32[6]{0:T(128)}, u32[]{:S(2)}) copy-start(s32[6]{0:T(128)} %lengths.1) | copy-start | bytes 76
  21.3 20.5 %copy-start.14 = (f32[2]{0:T(128)S(1)}, f32[2]{0:T(128)}, u32[]{:S(2)}) copy-start(f32[2]{0:T(128)} %offsets.1) | copy-start | bytes 28
  41.8 28.3 %copy-start.6 = (bf16[2048,64]{0,1:T(8,128)(2,1)S(1)}, bf16[2048,64]{0,1:T(8,128)(2,1)}, u32[]{:S(2)}) copy-start(bf16[2048,64]{0,1:T(8,128)(2,1)} %param.26) | copy-start | bytes 786436
  44.2 48.7 %copy-start.1 = (bf16[4096,128]{1,0:T(8,128)(2,1)S(1)}, bf16[4096,128]{1,0:T(8,128)(2,1)}, u32[]{:S(2)}) copy-start(bf16[4096,128]{1,0:T(8,128)(2,1)} %up_w.1) | copy-start | bytes 3145732
  44.2 48.7 %copy-start.2 = (bf16[128,4096]{1,0:T(8,128)(2,1)S(1)}, bf16[128,4096]{1,0:T(8,128)(2,1)}, u32[]{:S(2)}) copy-start(bf16[128,4096]{1,0:T(8,128)(2,1)} %down_w.1) | copy-start | bytes 3145732
  71.5 21.5 %copy-start.7 = (f32[4096]{0:T(1024)S(1)}, f32[4096]{0:T(1024)}, u32[]{:S(2)}) copy-start(f32[4096]{0:T(1024)} %param.27) | copy-start | bytes 49156

commit v3 on v2

--- a/solution.py
+++ b/solution.py
@@ -22,7 +22,7 @@
 floor_score = -1e30
 
 VMEM = pl.BlockSpec(memory_space=pltpu.VMEM)
-SMEM = pl.BlockSpec(memory_space=pltpu.SMEM)
+HBM = pl.BlockSpec(memory_space=pltpu.HBM)
 
 
 def call(body, out_shape, in_specs, scratch=(), flops=1 << 20):
@@ -55,29 +55,64 @@
     )
 
 
-def project(place, tokens, gain, query_w, key_w, value_w, forget_w, out):
+def kv_spot():
+    return lax.axis_index("kv_0") * lax.axis_size("kv_1") + lax.axis_index("kv_1")
+
+
+def project(
+    tokens_far, gain_far, query_far, key_far, value_far, forget_far, out,
+    tokens, gain, query_w, key_w, value_w, forget_w, dense, arrived,
+):
+    spot = kv_spot()
+    window = pl.ds(pl.multiple_of((spot // 2) * LANES, LANES), LANES)
+    copies = [
+        pltpu.make_async_copy(far, near, arrived.at[n])
+        for n, (far, near) in enumerate(
+            (
+                (query_far, query_w),
+                (tokens_far, tokens),
+                (gain_far, gain),
+                (key_far, key_w),
+                (value_far, value_w),
+                (forget_far.at[:, window], forget_w),
+            )
+        )
+    ]
+    for copy in copies:
+        copy.start()
+    for copy in copies[1:3]:
+        copy.wait()
     rows = tokens[...].astype(jnp.float32)
+    count, cols = rows.shape
     scaled = (rows * gain[...]).astype(jnp.bfloat16)
     wide = scaled.astype(jnp.float32)
-    gates = forget_w[...].astype(jnp.float32)
     square = jnp.sum(rows * rows, axis=1, keepdims=True)
     square_high = rounded(square)
+    for copy in copies[3:]:
+        copy.wait()
+    gates = forget_w[...].astype(jnp.float32)
+    gates = jnp.where(spot % 2 == 0, gates[:, :cols], gates[:, cols:])
     columns = [
         jnp.sum(wide * gates[n : n + 1, :], axis=1, keepdims=True) for n in range(gates.shape[0])
     ] + [square_high, square - square_high]
-    lane = lanes_of((rows.shape[0], LANES))
+    lane = lanes_of((count, LANES))
     extra = jnp.zeros(lane.shape, jnp.float32)
     for n, column in enumerate(columns):
-        extra = jnp.where(lane == n, column, extra)
-    line = jnp.concatenate(
-        (
-            dotted(scaled, query_w[...]),
-            dotted(scaled, key_w[...]),
-            dotted(scaled, value_w[...]),
-            extra,
-        ),
-        axis=1,
-    ).astype(jnp.bfloat16)
+        extra = jnp.where((lane == n) | (lane == n + HALF), column, extra)
+    third = count // 2
+    extra = jnp.where(lane[:third] < HALF, extra[:third], extra[third:])
+    copies[0].wait()
+    query = dotted(scaled, query_w[...])
+    pairs = query.shape[1] // LANES
+    stack = pairs * count
+    for j in range(pairs):
+        dense[pl.ds(j, count, stride=pairs), :] = query[:, LANES * j : LANES * (j + 1)]
+    dense[stack : stack + count, :] = dotted(scaled, key_w[...])
+    dense[stack + count : stack + 2 * count, :] = dotted(scaled, value_w[...])
+    dense[stack + 2 * count : stack + 2 * count + third, :] = extra
+    spare = stack + 2 * count + third
+    dense[spare:, :] = jnp.zeros((dense.shape[0] - spare, LANES), jnp.float32)
+    line = dense[...].astype(jnp.bfloat16)
     for k in range(RING):
         out[k] = line
 
@@ -95,24 +130,25 @@
         out[k] = line
 
 
-def attend(place, lengths, offsets, parts, keys, values, gate, out, turned):
+def attend(lengths, offsets, parts, keys, values, gate, out):
     count, positions = keys.shape[0], keys.shape[1]
-    pairs = turned.shape[0] // 8
-    spot, core = place[0], place[1]
+    spot = kv_spot()
     line = summed(parts)
-    width = pairs * LANES
-    extra = line[:, width + 2 * LANES :]
+    stack = line.shape[0] - 16
+    pairs = stack // count
+    tail = line[stack:]
+    extra = tail[2 * count : 2 * count + count // 2]
+    extra = jnp.concatenate((extra, pltpu.roll(extra, HALF, 1)), axis=0)
     row_scale = lax.rsqrt((extra[:, 4:5] + extra[:, 5:6]) / D + epsilon)
-    ready = rounded(line[:, : width + 2 * LANES] * row_scale)
-    new_key = ready[:, width : width + LANES]
-    new_value = ready[:, width + LANES :]
+    new_key = rounded(tail[:count] * row_scale)
+    new_value = rounded(tail[count : 2 * count] * row_scale)
     forget = []
     for n in range(2):
-        gate_in = jnp.where(core == 0, extra[:, n : n + 1], extra[:, n + 2 : n + 3])
-        z = gate_in * row_scale + offsets[n]
+        gate_in = jnp.where(
+            lax.axis_index("tp") == 0, extra[:, n : n + 1], extra[:, n + 2 : n + 3]
+        )
+        z = gate_in * row_scale + offsets[:, n : n + 1]
         forget.append(jnp.minimum(z, 0.0) - jnp.log1p(jnp.exp(-jnp.abs(z))))
-    for j in range(pairs):
-        turned[8 * j : 8 * j + count, :] = ready[:, LANES * j : LANES * (j + 1)]
     lane = lanes_of((pairs, LANES))
     row = lax.broadcasted_iota(jnp.int32, (pairs, LANES), 0)
     straight = (lane < HALF) == (row < pairs // 2)
@@ -122,7 +158,7 @@
     stats = jnp.zeros((8, LANES), jnp.float32)
     blocks = []
     for s in range(count):
-        both = turned[pl.ds(s, pairs, stride=8), :]
+        both = rounded(line[pairs * s : pairs * (s + 1)] * row_scale[s : s + 1, :])
         query = jnp.concatenate(
             (
                 jnp.where(straight, both, 0.0),
@@ -135,7 +171,7 @@
             jnp.broadcast_to(gate[s, n : n + 1, :] + forget[n][s : s + 1, :], (8, positions))
             for n in range(2)
         ]
-        live = place_of < lengths[s]
+        live = place_of < lengths[:, s : s + 1]
         score = jnp.where(live, score + jnp.concatenate(lines + lines, axis=0), floor_score)
         own = jnp.sum(query * new_key[s : s + 1, :], axis=1, keepdims=True) * HD ** (-0.5)
         own = jnp.where(first, own, floor_score)
@@ -209,7 +245,7 @@
         out[k] = line
 
 
-def finish(place, parts, tokens, out_w, out, turned):
+def finish(parts, tokens, out_w, out, turned):
     _, total, mixed, low = merged(parts)
     inverse = 1.0 / total
     for b, acc in enumerate(mixed):
@@ -220,7 +256,7 @@
         [turned[pl.ds(j, count, stride=pairs), :] for j in range(pairs)], axis=1
     ).astype(jnp.bfloat16)
     part = dotted(attended, out_w[...], 1)
-    part = part + jnp.where(place[1] == 0, tokens[...].astype(jnp.float32), 0.0)
+    part = part + jnp.where(lax.axis_index("tp") == 0, tokens[...].astype(jnp.float32), 0.0)
     third = count // 2
     piece = jnp.concatenate((part[:third], part[third:]), axis=1).astype(jnp.bfloat16)
     for k in range(out.shape[0]):
@@ -273,13 +309,13 @@
         out[8 * t : 8 * t + 8, :] = tile.astype(jnp.bfloat16)
 
 
-def close(place, parts, mid, out):
+def close(parts, mid, out):
     total = jnp.zeros((8, LANES), jnp.float32)
     for t in range(parts.shape[0] // 8):
         total = total + parts[8 * t : 8 * t + 8, :].astype(jnp.float32)
     pair = total[0:2] + total[2:4] + total[4:6] + total[6:8]
     count, width = out.shape
-    number = place[0] * 2 + place[1]
+    number = kv_spot() * 2 + lax.axis_index("tp")
     tile = mid[:, pl.ds(pl.multiple_of((number // 4) * LANES, LANES), LANES)]
     group = number % 4
     own = jnp.zeros((count, width), jnp.float32)
@@ -309,28 +345,29 @@
     down_weight,
 ):
     rows, cols = tokens.shape
-    spot = lax.axis_index(KV)
-    place = jnp.stack((spot, lax.axis_index("tp"))).astype(jnp.int32)
     bf16 = functools.partial(jax.ShapeDtypeStruct, dtype=jnp.bfloat16)
-    heads_wide = query_weight.shape[1]
-    line = heads_wide + 3 * LANES
-    gates = lax.dynamic_slice(
-        forget_weight.T, (0, spot * cols), (forget_weight.shape[1], cols)
-    )
-    x = call(project, bf16((RING, rows, line)), [SMEM] + [VMEM] * 6)(
-        place, tokens, attn_gain[None, :], query_weight, key_weight, value_weight, gates
-    )
+    stack = rows * query_weight.shape[1] // LANES
+    line = stack + 16
+    far = (tokens, attn_gain[None, :], query_weight, key_weight, value_weight, forget_weight.T)
+    near = [pltpu.VMEM(x.shape, x.dtype) for x in far[:5]]
+    x = call(
+        project,
+        bf16((RING, line, LANES)),
+        [HBM] * 6,
+        near
+        + [
+            pltpu.VMEM((forget_weight.shape[1], LANES), jnp.bfloat16),
+            pltpu.VMEM((line, LANES), jnp.float32),
+            pltpu.SemaphoreType.DMA((6,)),
+        ],
+    )(*[pltpu.with_memory_space_constraint(x, pltpu.HBM) for x in far])
     x = exchanged(x, "kv_1")
-    x = call(resend, bf16((RING, rows, line)), [VMEM])(x)
+    x = call(resend, bf16((RING, line, LANES)), [VMEM])(x)
     x = exchanged(x, "kv_0")
-    stack = rows * heads_wide // LANES
     packed = stack + 8
-    x = call(
-        attend,
-        bf16((RING, packed, LANES)),
-        [SMEM] * 3 + [VMEM] * 4,
-        [pltpu.VMEM((8 * heads_wide // LANES, LANES), jnp.float32)],
-    )(place, lengths, forget_offset, x, cache_keys, cache_values, gate_sum)
+    x = call(attend, bf16((RING, packed, LANES)), [VMEM] * 6)(
+        lengths[None, :], forget_offset[None, :], x, cache_keys, cache_values, gate_sum
+    )
     x = exchanged(x, "kv_1")
     x = call(combine, bf16((RING, packed, LANES)), [VMEM])(x)
     x = exchanged(x, "kv_0")
@@ -338,9 +375,9 @@
     x = call(
         finish,
         bf16((group, rows // 2, LANES)),
-        [SMEM] + [VMEM] * 3,
+        [VMEM] * 3,
         [pltpu.VMEM((stack, LANES), jnp.float32)],
-    )(place, x, tokens, out_weight.T)
+    )(x, tokens, out_weight.T)
     x = exchanged(x, KV_TP)
     mid, x = call(
         mix,
@@ -349,7 +386,7 @@
         [pltpu.VMEM((rows, D), jnp.float32)],
     )(x, mlp_gain[None, :], up_weight, down_weight)
     x = exchanged(x.reshape(group, 2, LANES), KV_TP).reshape(2 * group, LANES)
-    return call(close, bf16((rows, D // group)), [SMEM, VMEM, VMEM])(place, x, mid)
+    return call(close, bf16((rows, D // group)), [VMEM, VMEM])(x, mid)
 
 
 def solution(mesh):

time: 112 us -> 106 us (0.946)
  blocking collectives: 102 us -> 98.6 us
  local copies, waits for them, and re-layouts: 2.39 us -> 0.69 us
    all_to_all x6, blocking collectives: 102 us -> 98.6 us  [exchanged(): return lax.all_to_all(x, axes, split_axis=0, concat_axis=0, tiled=True)]
    unnamed x30 -> x20, local copies, waits for them, and re-layouts: 2.32 us -> 0.69 us
where the time goes in v3:
time: 106 us; the launch traced here: 105 us
  blocking collectives  98.6 us (93%)
  Pallas kernels  6.09 us (6%)
    all_to_all x6, blocking collectives, exchanged(): return lax.all_to_all(x, axes, split_axis=0, concat_axis=0, tiled=True)  98.6 us

profile of v3, /device:TPU:1, one launch (start us, length us, event | category | flops | bytes accessed | tf_op | source)
XLA Modules:
  0.0 105.5 jit_solution(9696405015771371894)
XLA Ops:
  0.0 1.2 %shard_map.145 = bf16[8,112,128]{2,1,0:T(8,128)(2,1)S(1)} custom-call(bf16[6,64]{1,0:T(8,128)(2,1)} %tokens.1, f32[1,64]{1,0:T(1,128)} %bitcast.15, bf16[64,2048]{1,0:T(8,128)(2,1)} %query_far.1, bf16[64,128]{1,0:T(8,128)(2,1)} %key_far.1, bf16[64,128]{1,0:T(8,128)(2,1)} %value_far.1, bf16[4,4096]{1,0:T(4,128)(2,1)} %bitcast.14), custom_call_target="tpu_custom_call" | custom-call | flops 1048576 | bytes 1048576 | tf_op jit(solution)/shard_map/pallas_call | solution.py:353
  1.2 16.3 %all_to_all.30.parts = bf16[8,112,128]{2,1,0:T(8,128)(2,1)S(1)} all-to-all(bf16[8,112,128]{2,1,0:T(8,128)(2,1)S(1)} %shard_map.145), channel_id=1, replica_groups=mesh['dp'=4,'kv_0'=8,'kv_1'=8,'tp'=2] {'kv_1'}, dimensions={0} | all-to-all | bytes 458752 | tf_op jit(solution)/shard_map/all_to_all | solution.py:49
  17.6 0.0 copy-start.2
  17.6 0.0 copy-start.3
  17.6 0.0 copy-start.6
  17.6 19.9 %all_to_all.31.parts = bf16[8,112,128]{2,1,0:T(8,128)(2,1)S(1)} all-to-all(bf16[8,112,128]{2,1,0:T(8,128)(2,1)S(1)} %shard_map.146), channel_id=1, replica_groups=mesh['dp'=4,'kv_0'=8,'kv_1'=8,'tp'=2] {'kv_0'}, dimensions={0} | all-to-all | bytes 458752 | tf_op jit(solution)/shard_map/all_to_all | solution.py:49
  37.5 0.0 copy-start.8
  37.6 0.0 copy-start.9
  37.6 0.0 copy-done.2
  37.6 0.0 copy-done.3
  37.6 0.0 copy-done.6
  37.6 0.6 copy-done.8
  38.2 0.0 copy-done.9
  38.2 0.0 copy-start.4
  38.2 0.0 copy-start.7
  38.2 2.0 %shard_map.147 = bf16[8,104,128]{2,1,0:T(8,128)(2,1)S(1)} custom-call(s32[1,6]{1,0:T(1,128)S(1)} %bitcast.12, f32[1,2]{1,0:T(1,128)S(1)} %bitcast.13, bf16[8,112,128]{2,1,0:T(8,128)(2,1)S(1)} %all_to_all.31.parts, bf16[6,256,128]{2,1,0:T(8,128)(2,1)S(1)} %copy-done.2, bf16[6,256,128]{2,1,0:T(8,128)(2,1)S(1)} %copy-done.3, f32[6,2,256]{2,1,0:T(2,128)S(1)} %copy-done.6), custom_call_target="tpu_custom_call" | custom-call | flops 1048576 | bytes 1048576 | tf_op jit(solution)/shard_map/pallas_call | solution.py:368
  40.2 0.0 copy-start
  40.2 0.0 copy-start.1
  40.2 11.6 %all_to_all.32.parts = bf16[8,104,128]{2,1,0:T(8,128)(2,1)S(1)} all-to-all(bf16[8,104,128]{2,1,0:T(8,128)(2,1)S(1)} %shard_map.147), channel_id=1, replica_groups=mesh['dp'=4,'kv_0'=8,'kv_1'=8,'tp'=2] {'kv_1'}, dimensions={0} | all-to-all | bytes 425984 | tf_op jit(solution)/shard_map/all_to_all | solution.py:49
  51.9 0.4 shard_map.148
  52.3 11.4 %all_to_all.33.parts = bf16[8,104,128]{2,1,0:T(8,128)(2,1)S(1)} all-to-all(bf16[8,104,128]{2,1,0:T(8,128)(2,1)S(1)} %shard_map.148), channel_id=1, replica_groups=mesh['dp'=4,'kv_0'=8,'kv_1'=8,'tp'=2] {'kv_0'}, dimensions={0} | all-to-all | bytes 425984 | tf_op jit(solution)/shard_map/all_to_all | solution.py:49
  63.7 0.0 copy-done.4
  63.7 0.0 copy-done.7
  63.7 0.7 shard_map.149
  64.4 0.0 copy-start.5
  64.5 22.8 %all_to_all.34.parts = bf16[128,3,128]{2,1,0:T(4,128)(2,1)S(1)} all-to-all(bf16[128,3,128]{2,1,0:T(4,128)(2,1)S(1)} %shard_map.149), channel_id=1, replica_groups=mesh['dp'=4,'kv_0'=8,'kv_1'=8,'tp'=2] {'kv_0','kv_1','tp'}, dimensions={0} | all-to-all | bytes 196608 | tf_op jit(solution)/shard_map/all_to_all | solution.py:49
  87.3 0.0 copy-done
  87.3 0.0 copy-done.1
  87.3 0.0 copy-done.5
  87.3 0.8 shard_map.150
  88.1 16.5 %all_to_all.35 = bf16[128,2,128]{2,1,0:T(2,128)(2,1)S(1)} all-to-all(bf16[128,2,128]{2,1,0:T(2,128)(2,1)S(1)} %bitcast.10), channel_id=1, replica_groups=mesh['dp'=4,'kv_0'=8,'kv_1'=8,'tp'=2] {'kv_0','kv_1','tp'}, dimensions={0} | all-to-all | bytes 131072 | tf_op jit(solution)/shard_map/all_to_all | solution.py:49
  104.6 0.9 shard_map.151
  (1 shorter events, 0.0 us)
Async XLA Ops:
  17.6 20.0 %copy-start.2 = (bf16[6,256,128]{2,1,0:T(8,128)(2,1)S(1)}, bf16[6,256,128]{2,1,0:T(8,128)(2,1)}, u32[]{:S(2)}) copy-start(bf16[6,256,128]{2,1,0:T(8,128)(2,1)} %keys.1) | copy-start | bytes 1179652
  17.6 20.0 %copy-start.3 = (bf16[6,256,128]{2,1,0:T(8,128)(2,1)S(1)}, bf16[6,256,128]{2,1,0:T(8,128)(2,1)}, u32[]{:S(2)}) copy-start(bf16[6,256,128]{2,1,0:T(8,128)(2,1)} %values.1) | copy-start | bytes 1179652
  17.6 20.0 %copy-start.6 = (f32[6,2,256]{2,1,0:T(2,128)S(1)}, f32[6,2,256]{2,1,0:T(2,128)}, u32[]{:S(2)}) copy-start(f32[6,2,256]{2,1,0:T(2,128)} %gate.1) | copy-start | bytes 36868
  37.5 0.7 copy-start.8
  37.6 0.7 copy-start.9
  38.2 25.5 %copy-start.4 = (bf16[2048,64]{0,1:T(8,128)(2,1)S(1)}, bf16[2048,64]{0,1:T(8,128)(2,1)}, u32[]{:S(2)}) copy-start(bf16[2048,64]{0,1:T(8,128)(2,1)} %param.26) | copy-start | bytes 786436
  38.2 25.5 %copy-start.7 = (bf16[6,64]{1,0:T(8,128)(2,1)S(1)}, bf16[6,64]{1,0:T(8,128)(2,1)}, u32[]{:S(2)}) copy-start(bf16[6,64]{1,0:T(8,128)(2,1)} %tokens.1) | copy-start | bytes 2308
  40.2 47.1 %copy-start = (bf16[4096,128]{1,0:T(8,128)(2,1)S(1)}, bf16[4096,128]{1,0:T(8,128)(2,1)}, u32[]{:S(2)}) copy-start(bf16[4096,128]{1,0:T(8,128)(2,1)} %up_w.1) | copy-start | bytes 3145732
  40.2 47.1 %copy-start.1 = (bf16[128,4096]{1,0:T(8,128)(2,1)S(1)}, bf16[128,4096]{1,0:T(8,128)(2,1)}, u32[]{:S(2)}) copy-start(bf16[128,4096]{1,0:T(8,128)(2,1)} %down_w.1) | copy-start | bytes 3145732
  64.4 22.8 %copy-start.5 = (f32[4096]{0:T(1024)S(1)}, f32[4096]{0:T(1024)}, u32[]{:S(2)}) copy-start(f32[4096]{0:T(1024)} %param.27) | copy-start | bytes 49156

commit v4 on v3

--- a/solution.py
+++ b/solution.py
@@ -60,7 +60,8 @@
 
 
 def project(
-    tokens_far, gain_far, query_far, key_far, value_far, forget_far, out,
+    tokens_far, gain_far, query_far, key_far, value_far, forget_far, lengths_far, offsets_far,
+    out, lengths, offsets,
     tokens, gain, query_w, key_w, value_w, forget_w, dense, arrived,
 ):
     spot = kv_spot()
@@ -75,6 +76,8 @@
                 (key_far, key_w),
                 (value_far, value_w),
                 (forget_far.at[:, window], forget_w),
+                (lengths_far, lengths),
+                (offsets_far, offsets),
             )
         )
     ]
@@ -137,57 +140,72 @@
     stack = line.shape[0] - 16
     pairs = stack // count
     tail = line[stack:]
-    extra = tail[2 * count : 2 * count + count // 2]
-    extra = jnp.concatenate((extra, pltpu.roll(extra, HALF, 1)), axis=0)
-    row_scale = lax.rsqrt((extra[:, 4:5] + extra[:, 5:6]) / D + epsilon)
+    third = count // 2
+    extra = tail[2 * count : 2 * count + third]
+    extra = jnp.concatenate((extra, extra), axis=0)
+    lane = lanes_of((count, LANES))
+    lane = lane - HALF * (lax.broadcasted_iota(jnp.int32, lane.shape, 0) // third)
+
+    def picked(first, last):
+        held = jnp.where((lane >= first) & (lane <= last), extra, 0.0)
+        return jnp.broadcast_to(jnp.sum(held, axis=1, keepdims=True), lane.shape)
+
+    row_scale = lax.rsqrt(picked(4, 5) / D + epsilon)
+    head = 2 * lax.axis_index("tp")
+    forget = []
+    for n in range(2):
+        z = picked(head + n, head + n) * row_scale + offsets[:, n : n + 1]
+        forget.append(jnp.minimum(z, 0.0) - jnp.log1p(jnp.exp(-jnp.abs(z))))
     new_key = rounded(tail[:count] * row_scale)
     new_value = rounded(tail[count : 2 * count] * row_scale)
-    forget = []
-    for n in range(2):
-        gate_in = jnp.where(
-            lax.axis_index("tp") == 0, extra[:, n : n + 1], extra[:, n + 2 : n + 3]
-        )
-        z = gate_in * row_scale + offsets[:, n : n + 1]
-        forget.append(jnp.minimum(z, 0.0) - jnp.log1p(jnp.exp(-jnp.abs(z))))
+    every = range(count)
     lane = lanes_of((pairs, LANES))
     row = lax.broadcasted_iota(jnp.int32, (pairs, LANES), 0)
     straight = (lane < HALF) == (row < pairs // 2)
     first = spot == 0
     place_of = spot * positions + lanes_of((1, positions))
+    live = [place_of < lengths[:, s : s + 1] for s in every]
+    both = [rounded(line[pairs * s : pairs * (s + 1)] * row_scale[s : s + 1, :]) for s in every]
+    rolled = [pltpu.roll(x, HALF, 1) for x in both]
+    queries = [
+        jnp.concatenate((jnp.where(straight, x, 0.0), jnp.where(straight, y, 0.0)), axis=0)
+        for x, y in zip(both, rolled)
+    ]
+    scores = [dotted(queries[s].astype(jnp.bfloat16), keys[s], 1) * HD ** (-0.5) for s in every]
+    owns = [
+        jnp.sum(queries[s] * new_key[s : s + 1, :], axis=1, keepdims=True) * HD ** (-0.5)
+        for s in every
+    ]
+    owns = [jnp.where(first, x, floor_score) for x in owns]
+    for s in every:
+        lines = [
+            jnp.broadcast_to(
+                gate[s, n : n + 1, :]
+                + jnp.concatenate([forget[n][s : s + 1, :]] * (positions // LANES), axis=1),
+                (8, positions),
+            )
+            for n in range(2)
+        ]
+        scores[s] = jnp.where(
+            live[s], scores[s] + jnp.concatenate(lines + lines, axis=0), floor_score
+        )
+    tops = [
+        rounded(jnp.maximum(jnp.max(scores[s], axis=1, keepdims=True), owns[s])) for s in every
+    ]
+    weights = [jnp.where(live[s], jnp.exp(scores[s] - tops[s]), 0.0) for s in every]
+    own_weights = [jnp.where(first, jnp.exp(owns[s] - tops[s]), 0.0) for s in every]
+    mixed = [dotted(weights[s].astype(jnp.bfloat16), values[s]) for s in every]
+    totals = [jnp.sum(weights[s], axis=1, keepdims=True) + own_weights[s] for s in every]
+    mixed = [mixed[s] + rounded(own_weights[s]) * new_value[s : s + 1, :] for s in every]
+    rolled = [pltpu.roll(x[pairs:], HALF, 1) for x in mixed]
+    blocks = [
+        jnp.where(straight, mixed[s][:pairs], rolled[s]).astype(jnp.bfloat16) for s in every
+    ]
     stat_lane = lanes_of((8, LANES))
     stats = jnp.zeros((8, LANES), jnp.float32)
-    blocks = []
-    for s in range(count):
-        both = rounded(line[pairs * s : pairs * (s + 1)] * row_scale[s : s + 1, :])
-        query = jnp.concatenate(
-            (
-                jnp.where(straight, both, 0.0),
-                jnp.where(straight, pltpu.roll(both, HALF, 1), 0.0),
-            ),
-            axis=0,
-        )
-        score = dotted(query.astype(jnp.bfloat16), keys[s], 1) * HD ** (-0.5)
-        lines = [
-            jnp.broadcast_to(gate[s, n : n + 1, :] + forget[n][s : s + 1, :], (8, positions))
-            for n in range(2)
-        ]
-        live = place_of < lengths[:, s : s + 1]
-        score = jnp.where(live, score + jnp.concatenate(lines + lines, axis=0), floor_score)
-        own = jnp.sum(query * new_key[s : s + 1, :], axis=1, keepdims=True) * HD ** (-0.5)
-        own = jnp.where(first, own, floor_score)
-        top = rounded(jnp.maximum(jnp.max(score, axis=1, keepdims=True), own))
-        weight = jnp.where(live, jnp.exp(score - top), 0.0)
-        own_weight = jnp.where(first, jnp.exp(own - top), 0.0)
-        total = jnp.sum(weight, axis=1, keepdims=True) + own_weight
-        mixed = dotted(weight.astype(jnp.bfloat16), values[s])
-        mixed = mixed + rounded(own_weight) * new_value[s : s + 1, :]
-        blocks.append(
-            jnp.where(straight, mixed[:pairs], pltpu.roll(mixed[pairs:], HALF, 1)).astype(
-                jnp.bfloat16
-            )
-        )
-        total_high = rounded(total)
-        for n, column in enumerate((top, total_high, total - total_high)):
+    for s in every:
+        total_high = rounded(totals[s])
+        for n, column in enumerate((tops[s], total_high, totals[s] - total_high)):
             for g in range(4):
                 stats = jnp.where(
                     stat_lane == 32 * g + 8 * n + s, column[8 * g : 8 * g + 8], stats
@@ -198,10 +216,11 @@
         out[k] = line
 
 
-def spread(compact, block, low):
+def spread(compact, block):
     s, half = divmod(block, 2)
     left, right = (s, 64 + s) if half == 0 else (96 + s, 32 + s)
-    return jnp.where(low, compact[:, left : left + 1], compact[:, right : right + 1])
+    source = jnp.where(lanes_of(compact.shape) < HALF, left, right)
+    return jnp.take_along_axis(compact, source, axis=1, mode="promise_in_bounds")
 
 
 def merged(parts):
@@ -217,20 +236,19 @@
             for scale, x in zip(scales, stats)
         ],
     )
-    low = lanes_of((8, LANES)) < HALF
     mixed = []
     for b in range(blocks):
         acc = jnp.zeros((8, LANES), jnp.float32)
         for k in range(RING):
             acc = acc + parts[k, 8 * b : 8 * b + 8, :].astype(jnp.float32) * spread(
-                scales[k], b, low
+                scales[k], b
             )
         mixed.append(acc)
-    return top, total, mixed, low
+    return top, total, mixed
 
 
 def combine(parts, out):
-    top, total, mixed, _ = merged(parts)
+    top, total, mixed = merged(parts)
     kind = lanes_of((8, LANES)) % 32
     total_high = rounded(total)
     stats = jnp.where(
@@ -246,10 +264,10 @@
 
 
 def finish(parts, tokens, out_w, out, turned):
-    _, total, mixed, low = merged(parts)
+    _, total, mixed = merged(parts)
     inverse = 1.0 / total
     for b, acc in enumerate(mixed):
-        turned[8 * b : 8 * b + 8, :] = rounded(acc * spread(inverse, b, low))
+        turned[8 * b : 8 * b + 8, :] = rounded(acc * spread(inverse, b))
     count = tokens.shape[0]
     pairs = turned.shape[0] // count
     attended = jnp.concatenate(
@@ -283,8 +301,8 @@
     scale = lax.rsqrt(jnp.sum(square, axis=1, keepdims=True) / D + epsilon)
     rows = mid[...]
     mid_out[...] = rows.astype(jnp.bfloat16)
-    normed = (rows * gain[...] * scale).astype(jnp.bfloat16)
-    hidden = jnp.square(jnp.maximum(dotted(normed, up_w[...]), 0.0))
+    gained = (rows * gain[...]).astype(jnp.bfloat16)
+    hidden = jnp.square(jnp.maximum(dotted(gained, up_w[...]) * scale, 0.0))
     hidden = jnp.concatenate((hidden, jnp.zeros((8 - count, LANES), jnp.float32)), axis=0)
     picked = jnp.concatenate(
         [
@@ -317,14 +335,11 @@
     count, width = out.shape
     number = kv_spot() * 2 + lax.axis_index("tp")
     tile = mid[:, pl.ds(pl.multiple_of((number // 4) * LANES, LANES), LANES)]
-    group = number % 4
-    own = jnp.zeros((count, width), jnp.float32)
-    for n in range(4):
-        own = jnp.where(
-            group == n, tile[:, width * n : width * (n + 1)].astype(jnp.float32), own
-        )
-    rows = [pair[r // 4 : r // 4 + 1, 32 * (r % 4) : 32 * (r % 4) + 32] for r in range(count)]
-    out[...] = (own + jnp.concatenate(rows, axis=0)).astype(jnp.bfloat16)
+    turn = lax.rem(4 - number % 4, 4) * 32
+    own = pltpu.roll(tile.astype(jnp.float32), turn, 1)
+    turned = [pair if n == 0 else pltpu.roll(pair, LANES - 32 * n, 1) for n in range(4)]
+    rows = [turned[r % 4][r // 4 : r // 4 + 1] for r in range(count)]
+    out[...] = (own + jnp.concatenate(rows, axis=0))[:, :width].astype(jnp.bfloat16)
 
 
 def shards(
@@ -348,17 +363,30 @@
     bf16 = functools.partial(jax.ShapeDtypeStruct, dtype=jnp.bfloat16)
     stack = rows * query_weight.shape[1] // LANES
     line = stack + 16
-    far = (tokens, attn_gain[None, :], query_weight, key_weight, value_weight, forget_weight.T)
+    far = (
+        tokens,
+        attn_gain[None, :],
+        query_weight,
+        key_weight,
+        value_weight,
+        forget_weight.T,
+        lengths[None, :],
+        forget_offset[None, :],
+    )
     near = [pltpu.VMEM(x.shape, x.dtype) for x in far[:5]]
-    x = call(
+    x, lengths, forget_offset = call(
         project,
-        bf16((RING, line, LANES)),
-        [HBM] * 6,
+        (
+            bf16((RING, line, LANES)),
+            jax.ShapeDtypeStruct(far[6].shape, far[6].dtype),
+            jax.ShapeDtypeStruct(far[7].shape, far[7].dtype),
+        ),
+        [HBM] * 8,
         near
         + [
             pltpu.VMEM((forget_weight.shape[1], LANES), jnp.bfloat16),
             pltpu.VMEM((line, LANES), jnp.float32),
-            pltpu.SemaphoreType.DMA((6,)),
+            pltpu.SemaphoreType.DMA((8,)),
         ],
     )(*[pltpu.with_memory_space_constraint(x, pltpu.HBM) for x in far])
     x = exchanged(x, "kv_1")
@@ -366,7 +394,7 @@
     x = exchanged(x, "kv_0")
     packed = stack + 8
     x = call(attend, bf16((RING, packed, LANES)), [VMEM] * 6)(
-        lengths[None, :], forget_offset[None, :], x, cache_keys, cache_values, gate_sum
+        lengths, forget_offset, x, cache_keys, cache_values, gate_sum
     )
     x = exchanged(x, "kv_1")
     x = call(combine, bf16((RING, packed, LANES)), [VMEM])(x)

time: 106 us -> 103 us (0.972)
  Pallas kernels: 6.09 us -> 4.25 us
    pallas_call x1, Pallas kernels: 2 us -> 0.66 us  [shards(): call(attend, bf16((RING, packed, LANES)), [VMEM] * 6)]
where the time goes in v4:
time: 103 us
  blocking collectives  98.6 us (96%)
  Pallas kernels  4.25 us (4%)
    all_to_all x6, blocking collectives, exchanged(): return lax.all_to_all(x, axes, split_axis=0, concat_axis=0, tiled=True)  98.6 us

profile of v4, /device:TPU:1, one launch (start us, length us, event | category | flops | bytes accessed | tf_op | source)
XLA Modules:
  0.0 103.0 jit_solution(6175185849613205808)
XLA Ops:
  0.0 1.3 %shard_map.145 = (bf16[8,112,128]{2,1,0:T(8,128)(2,1)S(1)}, s32[1,6]{1,0:T(1,128)S(1)}, f32[1,2]{1,0:T(1,128)S(1)}) custom-call(bf16[6,64]{1,0:T(8,128)(2,1)} %tokens.1, f32[1,64]{1,0:T(1,128)} %bitcast.13, bf16[64,2048]{1,0:T(8,128)(2,1)} %query_far.1, bf16[64,128]{1,0:T(8,128)(2,1)} %key_far.1, bf16[64,128]{1,0:T(8,128)(2,1)} %value_far.1, ...), custom_call_target="tpu_custom_call" | custom-call | flops 1048576 | bytes 1048576 | tf_op jit(solution)/shard_map/pallas_call | solution.py:377
  1.3 16.3 %all_to_all.30.parts = bf16[8,112,128]{2,1,0:T(8,128)(2,1)S(1)} all-to-all(bf16[8,112,128]{2,1,0:T(8,128)(2,1)S(1)} %get-tuple-element.12), channel_id=1, replica_groups=mesh['dp'=4,'kv_0'=8,'kv_1'=8,'tp'=2] {'kv_1'}, dimensions={0} | all-to-all | bytes 458752 | tf_op jit(solution)/shard_map/all_to_all | solution.py:49
  17.6 0.0 copy-start.2
  17.6 0.0 copy-start.3
  17.6 0.0 copy-start.6
  17.6 19.9 %all_to_all.31.parts = bf16[8,112,128]{2,1,0:T(8,128)(2,1)S(1)} all-to-all(bf16[8,112,128]{2,1,0:T(8,128)(2,1)S(1)} %shard_map.146), channel_id=1, replica_groups=mesh['dp'=4,'kv_0'=8,'kv_1'=8,'tp'=2] {'kv_0'}, dimensions={0} | all-to-all | bytes 458752 | tf_op jit(solution)/shard_map/all_to_all | solution.py:49
  37.6 0.0 copy-done.2
  37.6 0.0 copy-done.3
  37.6 0.0 copy-done.6
  37.6 0.0 copy-start.4
  37.6 0.0 copy-start.7
  37.6 0.7 shard_map.147
  38.2 0.0 copy-start
  38.3 0.0 copy-start.1
  38.3 11.6 %all_to_all.32.parts = bf16[8,104,128]{2,1,0:T(8,128)(2,1)S(1)} all-to-all(bf16[8,104,128]{2,1,0:T(8,128)(2,1)S(1)} %shard_map.147), channel_id=1, replica_groups=mesh['dp'=4,'kv_0'=8,'kv_1'=8,'tp'=2] {'kv_1'}, dimensions={0} | all-to-all | bytes 425984 | tf_op jit(solution)/shard_map/all_to_all | solution.py:49
  49.9 0.2 shard_map.148
  50.2 11.4 %all_to_all.33.parts = bf16[8,104,128]{2,1,0:T(8,128)(2,1)S(1)} all-to-all(bf16[8,104,128]{2,1,0:T(8,128)(2,1)S(1)} %shard_map.148), channel_id=1, replica_groups=mesh['dp'=4,'kv_0'=8,'kv_1'=8,'tp'=2] {'kv_0'}, dimensions={0} | all-to-all | bytes 425984 | tf_op jit(solution)/shard_map/all_to_all | solution.py:49
  61.6 0.0 copy-done.4
  61.6 0.0 copy-done.7
  61.6 0.7 shard_map.149
  62.3 0.0 copy-start.5
  62.3 22.8 %all_to_all.34.parts = bf16[128,3,128]{2,1,0:T(4,128)(2,1)S(1)} all-to-all(bf16[128,3,128]{2,1,0:T(4,128)(2,1)S(1)} %shard_map.149), channel_id=1, replica_groups=mesh['dp'=4,'kv_0'=8,'kv_1'=8,'tp'=2] {'kv_0','kv_1','tp'}, dimensions={0} | all-to-all | bytes 196608 | tf_op jit(solution)/shard_map/all_to_all | solution.py:49
  85.1 0.0 copy-done
  85.1 0.0 copy-done.1
  85.1 0.0 copy-done.5
  85.1 0.7 shard_map.150
  85.8 16.5 %all_to_all.35 = bf16[128,2,128]{2,1,0:T(2,128)(2,1)S(1)} all-to-all(bf16[128,2,128]{2,1,0:T(2,128)(2,1)S(1)} %bitcast.10), channel_id=1, replica_groups=mesh['dp'=4,'kv_0'=8,'kv_1'=8,'tp'=2] {'kv_0','kv_1','tp'}, dimensions={0} | all-to-all | bytes 131072 | tf_op jit(solution)/shard_map/all_to_all | solution.py:49
  102.3 0.7 shard_map.151
  (1 shorter events, 0.0 us)
Async XLA Ops:
  17.6 20.0 %copy-start.2 = (bf16[6,256,128]{2,1,0:T(8,128)(2,1)S(1)}, bf16[6,256,128]{2,1,0:T(8,128)(2,1)}, u32[]{:S(2)}) copy-start(bf16[6,256,128]{2,1,0:T(8,128)(2,1)} %keys.1) | copy-start | bytes 1179652
  17.6 20.0 %copy-start.3 = (bf16[6,256,128]{2,1,0:T(8,128)(2,1)S(1)}, bf16[6,256,128]{2,1,0:T(8,128)(2,1)}, u32[]{:S(2)}) copy-start(bf16[6,256,128]{2,1,0:T(8,128)(2,1)} %values.1) | copy-start | bytes 1179652
  17.6 19.9 %copy-start.6 = (f32[6,2,256]{2,1,0:T(2,128)S(1)}, f32[6,2,256]{2,1,0:T(2,128)}, u32[]{:S(2)}) copy-start(f32[6,2,256]{2,1,0:T(2,128)} %gate.1) | copy-start | bytes 36868
  37.6 24.0 %copy-start.4 = (bf16[2048,64]{0,1:T(8,128)(2,1)S(1)}, bf16[2048,64]{0,1:T(8,128)(2,1)}, u32[]{:S(2)}) copy-start(bf16[2048,64]{0,1:T(8,128)(2,1)} %param.26) | copy-start | bytes 786436
  37.6 24.0 %copy-start.7 = (bf16[6,64]{1,0:T(8,128)(2,1)S(1)}, bf16[6,64]{1,0:T(8,128)(2,1)}, u32[]{:S(2)}) copy-start(bf16[6,64]{1,0:T(8,128)(2,1)} %tokens.1) | copy-start | bytes 2308
  38.2 46.9 %copy-start = (bf16[4096,128]{1,0:T(8,128)(2,1)S(1)}, bf16[4096,128]{1,0:T(8,128)(2,1)}, u32[]{:S(2)}) copy-start(bf16[4096,128]{1,0:T(8,128)(2,1)} %up_w.1) | copy-start | bytes 3145732
  38.3 46.9 %copy-start.1 = (bf16[128,4096]{1,0:T(8,128)(2,1)S(1)}, bf16[128,4096]{1,0:T(8,128)(2,1)}, u32[]{:S(2)}) copy-start(bf16[128,4096]{1,0:T(8,128)(2,1)} %down_w.1) | copy-start | bytes 3145732
  62.3 22.8 %copy-start.5 = (f32[4096]{0:T(1024)S(1)}, f32[4096]{0:T(1024)}, u32[]{:S(2)}) copy-start(f32[4096]{0:T(1024)} %param.27) | copy-start | bytes 49156

commit v5 on v4

--- a/solution.py
+++ b/solution.py
@@ -17,6 +17,7 @@
 LANES = 128
 HALF = 64
 RING = 8
+RING_ORDER = (0, 4, 2, 6, 3, 7, 1, 5)
 
 epsilon = 1e-06
 floor_score = -1e30
@@ -45,8 +46,22 @@
     return x.astype(jnp.bfloat16).astype(jnp.float32)
 
 
-def exchanged(x, axes):
-    return lax.all_to_all(x, axes, split_axis=0, concat_axis=0, tiled=True)
+def exchanged(x, groups):
+    return lax.all_to_all(
+        x, KV_TP, split_axis=0, concat_axis=0, axis_index_groups=groups, tiled=True
+    )
+
+
+def ring_groups(along_last):
+    def member(fixed, moving, core):
+        first, last = (fixed, moving) if along_last else (moving, fixed)
+        return (first * RING + last) * 2 + core
+
+    return [
+        [member(fixed, moving, core) for moving in RING_ORDER]
+        for core in range(2)
+        for fixed in range(RING)
+    ]
 
 
 def dotted(a, b, b_dim=0):
@@ -389,16 +404,16 @@
             pltpu.SemaphoreType.DMA((8,)),
         ],
     )(*[pltpu.with_memory_space_constraint(x, pltpu.HBM) for x in far])
-    x = exchanged(x, "kv_1")
+    x = exchanged(x, ring_groups(True))
     x = call(resend, bf16((RING, line, LANES)), [VMEM])(x)
-    x = exchanged(x, "kv_0")
+    x = exchanged(x, ring_groups(False))
     packed = stack + 8
     x = call(attend, bf16((RING, packed, LANES)), [VMEM] * 6)(
         lengths, forget_offset, x, cache_keys, cache_values, gate_sum
     )
-    x = exchanged(x, "kv_1")
+    x = exchanged(x, ring_groups(True))
     x = call(combine, bf16((RING, packed, LANES)), [VMEM])(x)
-    x = exchanged(x, "kv_0")
+    x = exchanged(x, ring_groups(False))
     group = lax.axis_size(KV_TP)
     x = call(
         finish,
@@ -406,14 +421,14 @@
         [VMEM] * 3,
         [pltpu.VMEM((stack, LANES), jnp.float32)],
     )(x, tokens, out_weight.T)
-    x = exchanged(x, KV_TP)
+    x = exchanged(x, None)
     mid, x = call(
         mix,
         (bf16((rows, D)), bf16((2 * group, LANES))),
         [VMEM] * 4,
         [pltpu.VMEM((rows, D), jnp.float32)],
     )(x, mlp_gain[None, :], up_weight, down_weight)
-    x = exchanged(x.reshape(group, 2, LANES), KV_TP).reshape(2 * group, LANES)
+    x = exchanged(x.reshape(group, 2, LANES), None).reshape(2 * group, LANES)
     return call(close, bf16((rows, D // group)), [VMEM, VMEM])(x, mid)
 
 

time: 103 us -> 101 us (0.981)
  blocking collectives: 98.6 us -> 96.2 us
    all_to_all x6, blocking collectives: 98.6 us -> 96.2 us  [exchanged(): lax.all_to_all(x, KV_TP, split_axis=0, concat_axis=0, axis_index_groups=g...]
where the time goes in v5:
time: 101 us
  blocking collectives  96.2 us (95%)
  Pallas kernels  4.25 us (4%)
    all_to_all x6, blocking collectives, exchanged(): lax.all_to_all(x, KV_TP, split_axis=0, concat_axis=0, axis_index_groups=g...  96.2 us

profile of v5, /device:TPU:1, one launch (start us, length us, event | category | flops | bytes accessed | tf_op | source)
XLA Modules:
  0.0 100.6 jit_solution(15410391598641340113)
XLA Ops:
  0.0 1.3 %shard_map.145 = (bf16[8,112,128]{2,1,0:T(8,128)(2,1)S(1)}, s32[1,6]{1,0:T(1,128)S(1)}, f32[1,2]{1,0:T(1,128)S(1)}) custom-call(bf16[6,64]{1,0:T(8,128)(2,1)} %tokens.1, f32[1,64]{1,0:T(1,128)} %bitcast.13, bf16[64,2048]{1,0:T(8,128)(2,1)} %query_far.1, bf16[64,128]{1,0:T(8,128)(2,1)} %key_far.1, bf16[64,128]{1,0:T(8,128)(2,1)} %value_far.1, ...), custom_call_target="tpu_custom_call" | custom-call | flops 1048576 | bytes 1048576 | tf_op jit(solution)/shard_map/pallas_call | solution.py:392
  1.3 14.4 %all_to_all.30.parts = bf16[8,112,128]{2,1,0:T(8,128)(2,1)S(1)} all-to-all(bf16[8,112,128]{2,1,0:T(8,128)(2,1)S(1)} %get-tuple-element.12), channel_id=1, replica_groups={{0,8,4,12,6,14,2,10},{16,24,20,28,22,30,18,26},{32,40,36,44,38,46,34,42..., dimensions={0} | all-to-all | bytes 458752 | tf_op jit(solution)/shard_map/all_to_all | solution.py:50
  15.7 0.0 copy-start.2
  15.7 0.0 copy-start.3
  15.7 0.0 copy-start.6
  15.7 17.3 %all_to_all.31.parts = bf16[8,112,128]{2,1,0:T(8,128)(2,1)S(1)} all-to-all(bf16[8,112,128]{2,1,0:T(8,128)(2,1)S(1)} %shard_map.146), channel_id=1, replica_groups={{0,64,32,96,48,112,16,80},{2,66,34,98,50,114,18,82},{4,68,36,100,52,116..., dimensions={0} | all-to-all | bytes 458752 | tf_op jit(solution)/shard_map/all_to_all | solution.py:50
  33.0 0.0 copy-done.2
  33.0 0.0 copy-done.3
  33.0 0.0 copy-done.6
  33.0 0.0 copy-start.4
  33.0 0.0 copy-start.7
  33.0 0.7 shard_map.147
  33.7 0.0 copy-start
  33.7 0.0 copy-start.1
  33.7 12.0 %all_to_all.32.parts = bf16[8,104,128]{2,1,0:T(8,128)(2,1)S(1)} all-to-all(bf16[8,104,128]{2,1,0:T(8,128)(2,1)S(1)} %shard_map.147), channel_id=1, replica_groups={{0,8,4,12,6,14,2,10},{16,24,20,28,22,30,18,26},{32,40,36,44,38,46,34,42..., dimensions={0} | all-to-all | bytes 425984 | tf_op jit(solution)/shard_map/all_to_all | solution.py:50
  45.7 0.2 shard_map.148
  46.0 12.0 %all_to_all.33.parts = bf16[8,104,128]{2,1,0:T(8,128)(2,1)S(1)} all-to-all(bf16[8,104,128]{2,1,0:T(8,128)(2,1)S(1)} %shard_map.148), channel_id=1, replica_groups={{0,64,32,96,48,112,16,80},{2,66,34,98,50,114,18,82},{4,68,36,100,52,116..., dimensions={0} | all-to-all | bytes 425984 | tf_op jit(solution)/shard_map/all_to_all | solution.py:50
  58.0 0.0 copy-done.4
  58.0 0.0 copy-done.7
  58.0 0.7 shard_map.149
  58.7 0.0 copy-start.5
  58.7 24.0 %all_to_all.34.parts = bf16[128,3,128]{2,1,0:T(4,128)(2,1)S(1)} all-to-all(bf16[128,3,128]{2,1,0:T(4,128)(2,1)S(1)} %shard_map.149), channel_id=1, replica_groups=mesh['dp'=4,'kv_0'=8,'kv_1'=8,'tp'=2] {'kv_0','kv_1','tp'}, dimensions={0} | all-to-all | bytes 196608 | tf_op jit(solution)/shard_map/all_to_all | solution.py:50
  82.7 0.0 copy-done
  82.7 0.0 copy-done.1
  82.7 0.0 copy-done.5
  82.7 0.7 shard_map.150
  83.4 16.5 %all_to_all.35 = bf16[128,2,128]{2,1,0:T(2,128)(2,1)S(1)} all-to-all(bf16[128,2,128]{2,1,0:T(2,128)(2,1)S(1)} %bitcast.10), channel_id=1, replica_groups=mesh['dp'=4,'kv_0'=8,'kv_1'=8,'tp'=2] {'kv_0','kv_1','tp'}, dimensions={0} | all-to-all | bytes 131072 | tf_op jit(solution)/shard_map/all_to_all | solution.py:50
  99.9 0.7 shard_map.151
  (1 shorter events, 0.0 us)
Async XLA Ops:
  15.7 17.3 %copy-start.2 = (bf16[6,256,128]{2,1,0:T(8,128)(2,1)S(1)}, bf16[6,256,128]{2,1,0:T(8,128)(2,1)}, u32[]{:S(2)}) copy-start(bf16[6,256,128]{2,1,0:T(8,128)(2,1)} %keys.1) | copy-start | bytes 1179652
  15.7 17.3 %copy-start.3 = (bf16[6,256,128]{2,1,0:T(8,128)(2,1)S(1)}, bf16[6,256,128]{2,1,0:T(8,128)(2,1)}, u32[]{:S(2)}) copy-start(bf16[6,256,128]{2,1,0:T(8,128)(2,1)} %values.1) | copy-start | bytes 1179652
  15.7 17.3 %copy-start.6 = (f32[6,2,256]{2,1,0:T(2,128)S(1)}, f32[6,2,256]{2,1,0:T(2,128)}, u32[]{:S(2)}) copy-start(f32[6,2,256]{2,1,0:T(2,128)} %gate.1) | copy-start | bytes 36868
  33.0 25.0 %copy-start.4 = (bf16[2048,64]{0,1:T(8,128)(2,1)S(1)}, bf16[2048,64]{0,1:T(8,128)(2,1)}, u32[]{:S(2)}) copy-start(bf16[2048,64]{0,1:T(8,128)(2,1)} %param.26) | copy-start | bytes 786436
  33.0 25.0 %copy-start.7 = (bf16[6,64]{1,0:T(8,128)(2,1)S(1)}, bf16[6,64]{1,0:T(8,128)(2,1)}, u32[]{:S(2)}) copy-start(bf16[6,64]{1,0:T(8,128)(2,1)} %tokens.1) | copy-start | bytes 2308
  33.7 49.0 %copy-start = (bf16[4096,128]{1,0:T(8,128)(2,1)S(1)}, bf16[4096,128]{1,0:T(8,128)(2,1)}, u32[]{:S(2)}) copy-start(bf16[4096,128]{1,0:T(8,128)(2,1)} %up_w.1) | copy-start | bytes 3145732
  33.7 49.0 %copy-start.1 = (bf16[128,4096]{1,0:T(8,128)(2,1)S(1)}, bf16[128,4096]{1,0:T(8,128)(2,1)}, u32[]{:S(2)}) copy-start(bf16[128,4096]{1,0:T(8,128)(2,1)} %down_w.1) | copy-start | bytes 3145732
  58.7 24.1 %copy-start.5 = (f32[4096]{0:T(1024)S(1)}, f32[4096]{0:T(1024)}, u32[]{:S(2)}) copy-start(f32[4096]{0:T(1024)} %param.27) | copy-start | bytes 49156

commit v6 on v5

--- a/solution.py
+++ b/solution.py
@@ -17,7 +17,7 @@
 LANES = 128
 HALF = 64
 RING = 8
-RING_ORDER = (0, 4, 2, 6, 3, 7, 1, 5)
+RING_ORDER = (0, 2, 4, 6, 1, 3, 5, 7)
 
 epsilon = 1e-06
 floor_score = -1e30
@@ -291,7 +291,13 @@
     part = dotted(attended, out_w[...], 1)
     part = part + jnp.where(lax.axis_index("tp") == 0, tokens[...].astype(jnp.float32), 0.0)
     third = count // 2
-    piece = jnp.concatenate((part[:third], part[third:]), axis=1).astype(jnp.bfloat16)
+    upper, lower = part[:third], part[third:]
+    even = kv_spot() % 2 == 0
+    piece = jnp.where(
+        even,
+        jnp.concatenate((upper, lower), axis=1),
+        jnp.concatenate((lower, upper), axis=1),
+    ).astype(jnp.bfloat16)
     for k in range(out.shape[0]):
         out[k] = piece
 
@@ -309,8 +315,8 @@
             parts[4 * t + 2].astype(jnp.float32) + parts[4 * t + 3].astype(jnp.float32)
         )
         at = slice(LANES * t, LANES * (t + 1))
-        mid[:third, at] = jnp.where(low, a, pltpu.roll(b, HALF, 1))
-        mid[third:, at] = jnp.where(low, pltpu.roll(a, HALF, 1), b)
+        mid[:third, at] = jnp.where(low, a, b)
+        mid[third:, at] = pltpu.roll(jnp.where(low, b, a), HALF, 1)
         tile = mid[:, at]
         square = square + tile * tile
     scale = lax.rsqrt(jnp.sum(square, axis=1, keepdims=True) / D + epsilon)

time: 101 us -> 101 us (level)
  no operation moved by 1% of the time
where the time goes in v6:
time: 101 us; the launch traced here: 100 us
  blocking collectives  95.9 us (95%)
  Pallas kernels  4.25 us (4%)
    all_to_all x6, blocking collectives, exchanged(): lax.all_to_all(x, KV_TP, split_axis=0, concat_axis=0, axis_index_groups=g...  95.9 us

profile of v6, /device:TPU:1, one launch (start us, length us, event | category | flops | bytes accessed | tf_op | source)
XLA Modules:
  0.0 100.3 jit_solution(15756906034076630349)
XLA Ops:
  0.0 1.3 %shard_map.145 = (bf16[8,112,128]{2,1,0:T(8,128)(2,1)S(1)}, s32[1,6]{1,0:T(1,128)S(1)}, f32[1,2]{1,0:T(1,128)S(1)}) custom-call(bf16[6,64]{1,0:T(8,128)(2,1)} %tokens.1, f32[1,64]{1,0:T(1,128)} %bitcast.13, bf16[64,2048]{1,0:T(8,128)(2,1)} %query_far.1, bf16[64,128]{1,0:T(8,128)(2,1)} %key_far.1, bf16[64,128]{1,0:T(8,128)(2,1)} %value_far.1, ...), custom_call_target="tpu_custom_call" | custom-call | flops 1048576 | bytes 1048576 | tf_op jit(solution)/shard_map/pallas_call | solution.py:398
  1.3 15.0 %all_to_all.30.parts = bf16[8,112,128]{2,1,0:T(8,128)(2,1)S(1)} all-to-all(bf16[8,112,128]{2,1,0:T(8,128)(2,1)S(1)} %get-tuple-element.12), channel_id=1, replica_groups={{0,4,8,12,2,6,10,14},{16,20,24,28,18,22,26,30},{32,36,40,44,34,38,42,46..., dimensions={0} | all-to-all | bytes 458752 | tf_op jit(solution)/shard_map/all_to_all | solution.py:50
  16.3 0.0 copy-start.2
  16.3 0.0 copy-start.3
  16.3 0.0 copy-start.6
  16.3 17.4 %all_to_all.31.parts = bf16[8,112,128]{2,1,0:T(8,128)(2,1)S(1)} all-to-all(bf16[8,112,128]{2,1,0:T(8,128)(2,1)S(1)} %shard_map.146), channel_id=1, replica_groups={{0,32,64,96,16,48,80,112},{2,34,66,98,18,50,82,114},{4,36,68,100,20,52,..., dimensions={0} | all-to-all | bytes 458752 | tf_op jit(solution)/shard_map/all_to_all | solution.py:50
  33.7 0.0 copy-done.2
  33.7 0.0 copy-done.3
  33.7 0.0 copy-done.6
  33.7 0.0 copy-start.4
  33.7 0.0 copy-start.7
  33.8 0.7 shard_map.147
  34.4 0.0 copy-start
  34.4 0.0 copy-start.1
  34.4 12.3 %all_to_all.32.parts = bf16[8,104,128]{2,1,0:T(8,128)(2,1)S(1)} all-to-all(bf16[8,104,128]{2,1,0:T(8,128)(2,1)S(1)} %shard_map.147), channel_id=1, replica_groups={{0,4,8,12,2,6,10,14},{16,20,24,28,18,22,26,30},{32,36,40,44,34,38,42,46..., dimensions={0} | all-to-all | bytes 425984 | tf_op jit(solution)/shard_map/all_to_all | solution.py:50
  46.8 0.2 shard_map.148
  47.0 11.4 %all_to_all.33.parts = bf16[8,104,128]{2,1,0:T(8,128)(2,1)S(1)} all-to-all(bf16[8,104,128]{2,1,0:T(8,128)(2,1)S(1)} %shard_map.148), channel_id=1, replica_groups={{0,32,64,96,16,48,80,112},{2,34,66,98,18,50,82,114},{4,36,68,100,20,52,..., dimensions={0} | all-to-all | bytes 425984 | tf_op jit(solution)/shard_map/all_to_all | solution.py:50
  58.4 0.0 copy-done.4
  58.4 0.0 copy-done.7
  58.4 0.7 shard_map.149
  59.1 0.0 copy-start.5
  59.1 23.3 %all_to_all.34.parts = bf16[128,3,128]{2,1,0:T(4,128)(2,1)S(1)} all-to-all(bf16[128,3,128]{2,1,0:T(4,128)(2,1)S(1)} %shard_map.149), channel_id=1, replica_groups=mesh['dp'=4,'kv_0'=8,'kv_1'=8,'tp'=2] {'kv_0','kv_1','tp'}, dimensions={0} | all-to-all | bytes 196608 | tf_op jit(solution)/shard_map/all_to_all | solution.py:50
  82.4 0.0 copy-done
  82.4 0.0 copy-done.1
  82.4 0.0 copy-done.5
  82.4 0.7 shard_map.150
  83.1 16.5 %all_to_all.35 = bf16[128,2,128]{2,1,0:T(2,128)(2,1)S(1)} all-to-all(bf16[128,2,128]{2,1,0:T(2,128)(2,1)S(1)} %bitcast.10), channel_id=1, replica_groups=mesh['dp'=4,'kv_0'=8,'kv_1'=8,'tp'=2] {'kv_0','kv_1','tp'}, dimensions={0} | all-to-all | bytes 131072 | tf_op jit(solution)/shard_map/all_to_all | solution.py:50
  99.6 0.7 shard_map.151
  (1 shorter events, 0.0 us)
Async XLA Ops:
  16.3 17.4 %copy-start.2 = (bf16[6,256,128]{2,1,0:T(8,128)(2,1)S(1)}, bf16[6,256,128]{2,1,0:T(8,128)(2,1)}, u32[]{:S(2)}) copy-start(bf16[6,256,128]{2,1,0:T(8,128)(2,1)} %keys.1) | copy-start | bytes 1179652
  16.3 17.4 %copy-start.3 = (bf16[6,256,128]{2,1,0:T(8,128)(2,1)S(1)}, bf16[6,256,128]{2,1,0:T(8,128)(2,1)}, u32[]{:S(2)}) copy-start(bf16[6,256,128]{2,1,0:T(8,128)(2,1)} %values.1) | copy-start | bytes 1179652
  16.3 17.4 %copy-start.6 = (f32[6,2,256]{2,1,0:T(2,128)S(1)}, f32[6,2,256]{2,1,0:T(2,128)}, u32[]{:S(2)}) copy-start(f32[6,2,256]{2,1,0:T(2,128)} %gate.1) | copy-start | bytes 36868
  33.7 24.7 %copy-start.4 = (bf16[2048,64]{0,1:T(8,128)(2,1)S(1)}, bf16[2048,64]{0,1:T(8,128)(2,1)}, u32[]{:S(2)}) copy-start(bf16[2048,64]{0,1:T(8,128)(2,1)} %param.26) | copy-start | bytes 786436
  33.7 24.7 %copy-start.7 = (bf16[6,64]{1,0:T(8,128)(2,1)S(1)}, bf16[6,64]{1,0:T(8,128)(2,1)}, u32[]{:S(2)}) copy-start(bf16[6,64]{1,0:T(8,128)(2,1)} %tokens.1) | copy-start | bytes 2308
  34.4 48.0 %copy-start = (bf16[4096,128]{1,0:T(8,128)(2,1)S(1)}, bf16[4096,128]{1,0:T(8,128)(2,1)}, u32[]{:S(2)}) copy-start(bf16[4096,128]{1,0:T(8,128)(2,1)} %up_w.1) | copy-start | bytes 3145732
  34.4 48.0 %copy-start.1 = (bf16[128,4096]{1,0:T(8,128)(2,1)S(1)}, bf16[128,4096]{1,0:T(8,128)(2,1)}, u32[]{:S(2)}) copy-start(bf16[128,4096]{1,0:T(8,128)(2,1)} %down_w.1) | copy-start | bytes 3145732
  59.1 23.3 %copy-start.5 = (f32[4096]{0:T(1024)S(1)}, f32[4096]{0:T(1024)}, u32[]{:S(2)}) copy-start(f32[4096]{0:T(1024)} %param.27) | copy-start | bytes 49156

commit v7 on v6

--- a/solution.py
+++ b/solution.py
@@ -417,9 +417,9 @@
     x = call(attend, bf16((RING, packed, LANES)), [VMEM] * 6)(
         lengths, forget_offset, x, cache_keys, cache_values, gate_sum
     )
+    x = exchanged(x, ring_groups(False))
+    x = call(combine, bf16((RING, packed, LANES)), [VMEM])(x)
     x = exchanged(x, ring_groups(True))
-    x = call(combine, bf16((RING, packed, LANES)), [VMEM])(x)
-    x = exchanged(x, ring_groups(False))
     group = lax.axis_size(KV_TP)
     x = call(
         finish,

time: 101 us -> 101 us (level)
  no operation moved by 1% of the time
where the time goes in v7:
time: 101 us; the launch traced here: 100 us
  blocking collectives  95.9 us (95%)
  Pallas kernels  4.25 us (4%)
    all_to_all x6, blocking collectives, exchanged(): lax.all_to_all(x, KV_TP, split_axis=0, concat_axis=0, axis_index_groups=g...  95.9 us

profile of v7, /device:TPU:1, one launch (start us, length us, event | category | flops | bytes accessed | tf_op | source)
XLA Modules:
  0.0 100.3 jit_solution(8919887362920802955)
XLA Ops:
  0.0 1.3 %shard_map.145 = (bf16[8,112,128]{2,1,0:T(8,128)(2,1)S(1)}, s32[1,6]{1,0:T(1,128)S(1)}, f32[1,2]{1,0:T(1,128)S(1)}) custom-call(bf16[6,64]{1,0:T(8,128)(2,1)} %tokens.1, f32[1,64]{1,0:T(1,128)} %bitcast.13, bf16[64,2048]{1,0:T(8,128)(2,1)} %query_far.1, bf16[64,128]{1,0:T(8,128)(2,1)} %key_far.1, bf16[64,128]{1,0:T(8,128)(2,1)} %value_far.1, ...), custom_call_target="tpu_custom_call" | custom-call | flops 1048576 | bytes 1048576 | tf_op jit(solution)/shard_map/pallas_call | solution.py:398
  1.3 15.0 %all_to_all.30.parts = bf16[8,112,128]{2,1,0:T(8,128)(2,1)S(1)} all-to-all(bf16[8,112,128]{2,1,0:T(8,128)(2,1)S(1)} %get-tuple-element.12), channel_id=1, replica_groups={{0,4,8,12,2,6,10,14},{16,20,24,28,18,22,26,30},{32,36,40,44,34,38,42,46..., dimensions={0} | all-to-all | bytes 458752 | tf_op jit(solution)/shard_map/all_to_all | solution.py:50
  16.3 0.0 copy-start.2
  16.3 0.0 copy-start.3
  16.3 0.0 copy-start.6
  16.3 17.4 %all_to_all.31.parts = bf16[8,112,128]{2,1,0:T(8,128)(2,1)S(1)} all-to-all(bf16[8,112,128]{2,1,0:T(8,128)(2,1)S(1)} %shard_map.146), channel_id=1, replica_groups={{0,32,64,96,16,48,80,112},{2,34,66,98,18,50,82,114},{4,36,68,100,20,52,..., dimensions={0} | all-to-all | bytes 458752 | tf_op jit(solution)/shard_map/all_to_all | solution.py:50
  33.7 0.0 copy-done.2
  33.7 0.0 copy-done.3
  33.7 0.0 copy-done.6
  33.7 0.0 copy-start.4
  33.7 0.0 copy-start.7
  33.8 0.7 shard_map.147
  34.4 0.0 copy-start
  34.4 0.0 copy-start.1
  34.4 10.7 %all_to_all.32.parts = bf16[8,104,128]{2,1,0:T(8,128)(2,1)S(1)} all-to-all(bf16[8,104,128]{2,1,0:T(8,128)(2,1)S(1)} %shard_map.147), channel_id=1, replica_groups={{0,32,64,96,16,48,80,112},{2,34,66,98,18,50,82,114},{4,36,68,100,20,52,..., dimensions={0} | all-to-all | bytes 425984 | tf_op jit(solution)/shard_map/all_to_all | solution.py:50
  45.1 0.2 shard_map.148
  45.4 13.1 %all_to_all.33.parts = bf16[8,104,128]{2,1,0:T(8,128)(2,1)S(1)} all-to-all(bf16[8,104,128]{2,1,0:T(8,128)(2,1)S(1)} %shard_map.148), channel_id=1, replica_groups={{0,4,8,12,2,6,10,14},{16,20,24,28,18,22,26,30},{32,36,40,44,34,38,42,46..., dimensions={0} | all-to-all | bytes 425984 | tf_op jit(solution)/shard_map/all_to_all | solution.py:50
  58.4 0.0 copy-done.4
  58.4 0.0 copy-done.7
  58.4 0.7 shard_map.149
  59.1 0.0 copy-start.5
  59.1 23.3 %all_to_all.34.parts = bf16[128,3,128]{2,1,0:T(4,128)(2,1)S(1)} all-to-all(bf16[128,3,128]{2,1,0:T(4,128)(2,1)S(1)} %shard_map.149), channel_id=1, replica_groups=mesh['dp'=4,'kv_0'=8,'kv_1'=8,'tp'=2] {'kv_0','kv_1','tp'}, dimensions={0} | all-to-all | bytes 196608 | tf_op jit(solution)/shard_map/all_to_all | solution.py:50
  82.4 0.0 copy-done
  82.4 0.0 copy-done.1
  82.4 0.0 copy-done.5
  82.4 0.7 shard_map.150
  83.1 16.5 %all_to_all.35 = bf16[128,2,128]{2,1,0:T(2,128)(2,1)S(1)} all-to-all(bf16[128,2,128]{2,1,0:T(2,128)(2,1)S(1)} %bitcast.10), channel_id=1, replica_groups=mesh['dp'=4,'kv_0'=8,'kv_1'=8,'tp'=2] {'kv_0','kv_1','tp'}, dimensions={0} | all-to-all | bytes 131072 | tf_op jit(solution)/shard_map/all_to_all | solution.py:50
  99.6 0.7 shard_map.151
  (1 shorter events, 0.0 us)
Async XLA Ops:
  16.3 17.4 %copy-start.2 = (bf16[6,256,128]{2,1,0:T(8,128)(2,1)S(1)}, bf16[6,256,128]{2,1,0:T(8,128)(2,1)}, u32[]{:S(2)}) copy-start(bf16[6,256,128]{2,1,0:T(8,128)(2,1)} %keys.1) | copy-start | bytes 1179652
  16.3 17.4 %copy-start.3 = (bf16[6,256,128]{2,1,0:T(8,128)(2,1)S(1)}, bf16[6,256,128]{2,1,0:T(8,128)(2,1)}, u32[]{:S(2)}) copy-start(bf16[6,256,128]{2,1,0:T(8,128)(2,1)} %values.1) | copy-start | bytes 1179652
  16.3 17.4 %copy-start.6 = (f32[6,2,256]{2,1,0:T(2,128)S(1)}, f32[6,2,256]{2,1,0:T(2,128)}, u32[]{:S(2)}) copy-start(f32[6,2,256]{2,1,0:T(2,128)} %gate.1) | copy-start | bytes 36868
  33.7 24.7 %copy-start.4 = (bf16[2048,64]{0,1:T(8,128)(2,1)S(1)}, bf16[2048,64]{0,1:T(8,128)(2,1)}, u32[]{:S(2)}) copy-start(bf16[2048,64]{0,1:T(8,128)(2,1)} %param.26) | copy-start | bytes 786436
  33.7 24.7 %copy-start.7 = (bf16[6,64]{1,0:T(8,128)(2,1)S(1)}, bf16[6,64]{1,0:T(8,128)(2,1)}, u32[]{:S(2)}) copy-start(bf16[6,64]{1,0:T(8,128)(2,1)} %tokens.1) | copy-start | bytes 2308
  34.4 48.0 %copy-start = (bf16[4096,128]{1,0:T(8,128)(2,1)S(1)}, bf16[4096,128]{1,0:T(8,128)(2,1)}, u32[]{:S(2)}) copy-start(bf16[4096,128]{1,0:T(8,128)(2,1)} %up_w.1) | copy-start | bytes 3145732
  34.4 48.0 %copy-start.1 = (bf16[128,4096]{1,0:T(8,128)(2,1)S(1)}, bf16[128,4096]{1,0:T(8,128)(2,1)}, u32[]{:S(2)}) copy-start(bf16[128,4096]{1,0:T(8,128)(2,1)} %down_w.1) | copy-start | bytes 3145732
  59.1 23.3 %copy-start.5 = (f32[4096]{0:T(1024)S(1)}, f32[4096]{0:T(1024)}, u32[]{:S(2)}) copy-start(f32[4096]{0:T(1024)} %param.27) | copy-start | bytes 49156
